TPU v7x, 256 devices: a whole 4x4x8 slice. The times are simulated.
256 devices in a mesh: rep: 2 (over z_hi), fs: 16 (over z_lo, y), tp: 8 (over x, core).
Axes of the slice: x: 4, y: 4, z: 8 (z_hi: 2, z_lo: 4; z = z_hi * 4 + z_lo), core: 2. Of those that a mesh axis runs over, the one named last changes fastest.
Arguments:
- block_input: bfloat16 [16384, 2048], P(('rep', 'fs', 'tp')), may hold values from -6 to 6
- pre_gain: float32 [2048], replicated, may hold values from 0.1 to 1.9
- post_gain: float32 [2048], replicated, may hold values from 0.1 to 1.9
- gate_saved: bfloat16 [16384, 5632], P(('rep', 'fs'), 'tp'), may hold values from -8 to 8
- up_saved: bfloat16 [16384, 5632], P(('rep', 'fs'), 'tp'), may hold values from -6 to 6
- branch_saved: bfloat16 [16384, 2048], P(('rep', 'fs', 'tp')), may hold values from -6 to 6
- out_cotangent: bfloat16 [16384, 2048], P(('rep', 'fs', 'tp')), may hold values from -24 to 24
- gate_weight: bfloat16 [2048, 5632], P('fs', 'tp'), may hold values from -0.125 to 0.125
- up_weight: bfloat16 [2048, 5632], P('fs', 'tp'), may hold values from -0.125 to 0.125
- down_weight: bfloat16 [2048, 5632], P('fs', 'tp'), may hold values from -0.078125 to 0.078125
Outputs:
- input_grad: bfloat16 [16384, 2048], P(('rep', 'fs', 'tp'))
- gate_grad: float32 [2048, 5632], P('fs', 'tp')
- up_grad: float32 [2048, 5632], P('fs', 'tp')
- down_grad: float32 [2048, 5632], P('fs', 'tp')
All inputs are finite; a program needn't handle non-finite values.
Results may differ from a plain program's by a relative error of at most 0.018.
Values may be sent and summed in bfloat16 or wider, within the bound.
A program may use at most 128 MiB of HBM per device.

v0:
```python
import jax
import jax.numpy as jnp
from jax import lax
from jax.sharding import PartitionSpec as P

eps = 1e-06


def side_by_side(arrays, axis, dim, along):
    widths = [a.shape[along] for a in arrays]
    both = jnp.concatenate(arrays, axis=along)
    whole = lax.all_gather(both, axis, axis=dim, tiled=True)
    return tuple(jnp.split(whole, [sum(widths[:k]) for k in range(1, len(widths))], axis=along))


def joined_along(blocks, dim):
    lengths = list(blocks.shape[1:])
    lengths[dim] *= blocks.shape[0]
    return jnp.moveaxis(blocks, 0, dim).reshape(lengths)


def gather_together(arrays, axis, dims):
    flat = jnp.concatenate([a.reshape(-1) for a in arrays])
    lines, at, finished = (lax.all_gather(flat, axis), 0, [])
    for a, dim in zip(arrays, dims):
        blocks = lines[:, at : at + a.size].reshape(-1, *a.shape)
        finished.append(joined_along(blocks, dim))
        at += a.size
    return tuple(finished)


def split_up(shard, dim, size):
    lengths = shard.shape
    blocks = shard.reshape(*lengths[:dim], size, lengths[dim] // size, *lengths[dim + 1 :])
    return jnp.moveaxis(blocks, dim, 0)


def sum_at_owner(shard, axis, dim):
    size = lax.axis_size(axis)
    blocks = lax.all_to_all(split_up(shard, dim, size), axis, 0, 0, tiled=True)
    return jnp.sum(blocks.astype(jnp.float32), axis=0)


def side_by_side_2(arrays, axis, dim, along):
    widths = [a.shape[along] for a in arrays]
    both = jnp.concatenate(arrays, axis=along)
    whole = lax.psum_scatter(both, axis, scatter_dimension=dim, tiled=True)
    return tuple(jnp.split(whole, [sum(widths[:k]) for k in range(1, len(widths))], axis=along))


def copy_for_each(shard, axis):
    size = lax.axis_size(axis)
    return lax.all_to_all(
        jnp.broadcast_to(shard[None], (size, *shard.shape)), axis, 0, 0, tiled=True
    )


def of_everyone(shard, axis):
    everything = copy_for_each(shard, axis)
    return jnp.sum(everything.astype(jnp.float32), axis=0)


def contract_rows(left, right):
    return lax.dot_general(
        left, right, (((0,), (0,)), ((), ())), preferred_element_type=jnp.float32
    )


def contract_cols(left, right):
    return lax.dot_general(
        left, right, (((1,), (1,)), ((), ())), preferred_element_type=jnp.float32
    )


def per_device(
    block_input,
    pre_gain,
    post_gain,
    gate_saved,
    up_saved,
    branch_saved,
    out_cotangent,
    gate_weight,
    up_weight,
    down_weight,
):
    xfull = block_input.astype(jnp.float32)
    inv_x = lax.rsqrt(jnp.mean(xfull * xfull, axis=-1, keepdims=True) + eps)
    normed = (xfull * inv_x * pre_gain).astype(jnp.bfloat16)
    branch = branch_saved.astype(jnp.float32)
    inv_b = lax.rsqrt(jnp.mean(branch * branch, axis=-1, keepdims=True) + eps)
    upstream = 0.5 * out_cotangent.astype(jnp.float32) * post_gain
    branch_grad = (
        inv_b * upstream - branch * inv_b**3 * jnp.mean(upstream * branch, axis=-1, keepdims=True)
    ).astype(jnp.bfloat16)
    gate_full, up_full, down_full = side_by_side((gate_weight, up_weight, down_weight), "fs", 0, 1)
    normed_rows, branch_rows = gather_together((normed, branch_grad), "tp", (0, 0))
    gate_f = gate_saved.astype(jnp.float32)
    up_f = up_saved.astype(jnp.float32)
    sigma = jax.nn.sigmoid(gate_f)
    silu_gate = gate_f * sigma
    hidden = (silu_gate * up_f).astype(jnp.bfloat16)
    hidden_grad = jnp.dot(branch_rows, down_full, preferred_element_type=jnp.float32)
    gate_cot = (hidden_grad * up_f * sigma * (1.0 + gate_f * (1.0 - sigma))).astype(jnp.bfloat16)
    up_cot = (hidden_grad * silu_gate).astype(jnp.bfloat16)
    normed_grad = sum_at_owner(
        (contract_cols(gate_cot, gate_full) + contract_cols(up_cot, up_full)).astype(jnp.bfloat16),
        "tp",
        0,
    )
    scaled = normed_grad * pre_gain
    input_grad = (
        out_cotangent.astype(jnp.float32)
        + inv_x * scaled
        - xfull * inv_x**3 * jnp.mean(scaled * xfull, axis=-1, keepdims=True)
    )
    gate_sum = contract_rows(normed_rows, gate_cot)
    up_sum = contract_rows(normed_rows, up_cot)
    down_sum = contract_rows(branch_rows, hidden)
    shards = tuple(
        (
            part.astype(jnp.float32)
            for part in side_by_side_2(
                (
                    gate_sum.astype(jnp.bfloat16),
                    up_sum.astype(jnp.bfloat16),
                    down_sum.astype(jnp.bfloat16),
                ),
                "fs",
                0,
                1,
            )
        )
    )
    gate_grad, up_grad, down_grad = (
        of_everyone(shards[0].astype(jnp.bfloat16), "rep").astype(jnp.float32),
        of_everyone(shards[1].astype(jnp.bfloat16), "rep").astype(jnp.float32),
        of_everyone(shards[2].astype(jnp.bfloat16), "rep").astype(jnp.float32),
    )
    return (input_grad.astype(jnp.bfloat16), gate_grad, up_grad, down_grad)


def solution(mesh):
    return jax.shard_map(
        per_device,
        mesh=mesh,
        in_specs=(
            P(("rep", "fs", "tp"), None),
            P(),
            P(),
            P(("rep", "fs"), "tp"),
            P(("rep", "fs"), "tp"),
            P(("rep", "fs", "tp"), None),
            P(("rep", "fs", "tp"), None),
            P("fs", "tp"),
            P("fs", "tp"),
            P("fs", "tp"),
        ),
        out_specs=(P(("rep", "fs", "tp"), None), P("fs", "tp"), P("fs", "tp"), P("fs", "tp")),
        check_vma=False,
    )
```

profile of v0, /device:TPU:6, one launch (start us, length us, event | category | flops | bytes accessed | tf_op | source)
XLA Modules:
  0.0 367.6 jit_solution(12679925552836936272)
XLA Ops:
  7.2 0.0 all-gather.6.cloned.1.call-start
  7.2 0.7 broadcast_multiply_fusion
  8.0 1.2 fusion.19
  9.3 1.3 fusion.28
  10.6 1.1 fusion.22
  11.8 0.1 fusion.27
  12.0 0.8 pad_maximum_fusion.2
  12.8 0.0 all-gather.6.cloned.1.call-update
  12.8 0.0 all-gather.4.cloned.1.call-start
  12.9 0.9 pad_maximum_fusion.1
  13.8 0.0 reduce-scatter.4.cloned.1.call-start
  13.8 34.8 %all-gather.6.cloned.1.call-done = bf16[2097152]{0:T(1024)(128)(2,1)} async-done(((bf16[262144]{0:T(1024)(128)(2,1)}), bf16[2097152]{0:T(1024)(128)(2,1)}) %all-gather.6.cloned.1.call-update) | async-done | bytes 4194320 | tf_op jit(solution)/shard_map/all_gather | solution.py:24
  48.6 5.9 %reshape.61 = bf16[8,262144]{1,0:T(8,128)(2,1)} reshape(bf16[2097152]{0:T(1024)(128)(2,1)} %all-gather.6.cloned.1.call-done) | data formatting | bytes 8388608 | tf_op jit(solution)/shard_map/all_gather | solution.py:24
  54.5 3.8 %fusion.30 = (bf16[8,131072]{1,0:T(8,128)(2,1)S(1)}, bf16[8,131072]{1,0:T(8,128)(2,1)}) fusion(bf16[8,262144]{1,0:T(8,128)(2,1)} %reshape.61), kind=kLoop, calls=%fused_computation.62 | loop fusion | bytes 8388608 | tf_op jit(solution)/shard_map/slice | solution.py:26
  58.4 3.9 %reshape_reshape.6 = bf16[512,2048]{1,0:T(8,128)(2,1)} reshape(bf16[8,131072]{1,0:T(8,128)(2,1)} %get-tuple-element.7) | data formatting | bytes 4194304 | tf_op jit(solution)/shard_map/reshape;reshape | solution.py:19
  62.2 2.3 reshape_reshape.7
  64.5 5.5 %convolution_convert_fusion = bf16[2048,704]{0,1:T(8,128)(2,1)} fusion(bf16[512,2048]{1,0:T(8,128)(2,1)} %reshape_reshape.6, bf16[512,704]{0,1:T(8,128)(2,1)} %param.14, bf16[512,704]{0,1:T(8,128)(2,1)} %param.13), kind=kOutput, calls=%fused_computation.3 | convolution fusion | flops 1480720384 | bytes 6422528 | tf_op jit(solution)/shard_map/dot_general | solution.py:64
  70.0 107.9 %all-gather.4.cloned.1.call-done = bf16[2048,2112]{0,1:T(8,128)(2,1)} async-done(((bf16[128,2112]{0,1:T(8,128)(2,1)}), bf16[2048,2112]{0,1:T(8,128)(2,1)}) %all-gather.4.cloned.1.call-update) | async-done | bytes 8650768 | tf_op jit(solution)/shard_map/all_gather | solution.py:12
  177.9 4.9 %fusion.7 = (bf16[512,704]{0,1:T(8,128)(2,1)S(1)}, f32[512,704]{0,1:T(8,128)S(1)}) fusion(bf16[512,704]{0,1:T(8,128)(2,1)} %param.14, bf16[512,704]{0,1:T(8,128)(2,1)} %param.13, bf16[512,2048]{1,0:T(8,128)(2,1)} %reshape_reshape.6, bf16[2048,2112]{0,1:T(8,128)(2,1)} %all-gather.4.cloned.1.call-done), kind=kOutput, calls=%fused_computation.18 | convolution fusion | flops 1480720384 | bytes 8585216 | tf_op jit(solution)/shard_map/dot_general | solution.py:103
  182.9 1.7 convolution_convert_fusion.1
  184.7 1.7 convolution_convert_fusion.2
  186.4 0.1 copy-done.1
  186.5 4.3 %pad_maximum_fusion = bf16[2048,2112]{0,1:T(8,128)(2,1)} fusion(bf16[2048,704]{0,1:T(8,128)(2,1)S(1)} %copy-done.1, bf16[2048,704]{0,1:T(8,128)(2,1)S(1)} %convolution_convert_fusion.1, bf16[2048,704]{0,1:T(8,128)(2,1)S(1)} %convolution_convert_fusion.2), kind=kLoop, calls=%fused_computation | loop fusion | flops 25952256 | bytes 17301504 | tf_op jit(solution)/shard_map/concatenate | solution.py:46
  190.8 11.7 %copy.17 = bf16[2048,2112]{1,0:T(8,128)(2,1)} copy(bf16[2048,2112]{0,1:T(8,128)(2,1)} %pad_maximum_fusion) | data formatting | bytes 17301504
  202.5 1.1 copy-done.5
  203.6 3.8 %fusion.1 = f32[512,2048]{1,0:T(8,128)S(1)} fusion(bf16[512,704]{0,1:T(8,128)(2,1)S(1)} %copy-done.5, bf16[2048,2112]{0,1:T(8,128)(2,1)} %all-gather.4.cloned.1.call-done), kind=kOutput, calls=%fused_computation.7 | convolution fusion | flops 1476395008 | bytes 7798784 | tf_op jit(solution)/shard_map/dot_general | solution.py:70
  207.5 5.3 %add_convert_fusion = bf16[512,2048]{1,0:T(8,128)(2,1)} fusion(f32[512,2048]{1,0:T(8,128)S(1)} %fusion.1, bf16[2048,2112]{0,1:T(8,128)(2,1)} %all-gather.4.cloned.1.call-done, f32[512,704]{0,1:T(8,128)S(1)} %copy-done.13, bf16[512,704]{0,1:T(8,128)(2,1)S(1)} %copy-done.11), kind=kOutput, calls=%fused_computation.2 | convolution fusion | flops 1481015296 | bytes 11337728 | tf_op jit(solution)/shard_map/dot_general | solution.py:70
  212.7 4.8 %all-to-all-start = ((bf16[8,64,2048]{2,1,0:T(8,128)(2,1)}), bf16[8,64,2048]{2,1,0:T(8,128)(2,1)S(1)}, u32[]{:S(2)}, u32[]{:S(2)}) async-start(bf16[8,64,2048]{2,1,0:T(8,128)(2,1)} %bitcast.14), calls=%async_computation | async-start | bytes 4194304 | tf_op jit(solution)/shard_map/all_to_all | solution.py:40
  217.5 96.6 %reduce-scatter.4.cloned.1.call-done = bf16[128,2112]{1,0:T(8,128)(2,1)} async-done(((bf16[2048,2112]{1,0:T(8,128)(2,1)}), bf16[128,2112]{1,0:T(8,128)(2,1)}) %reduce-scatter.4.cloned.1.call-update) | async-done | bytes 540688
  314.1 1.9 fusion.31
  316.1 0.2 copy.19
  316.3 0.8 broadcast_in_dim.6
  317.0 4.2 %all-to-all-start.1 = ((bf16[2,128,704]{1,2,0:T(8,128)(2,1)}), bf16[2,128,704]{1,2,0:T(8,128)(2,1)S(1)}, u32[]{:S(2)}, u32[]{:S(2)}) async-start(bf16[2,128,704]{1,2,0:T(8,128)(2,1)} %broadcast_in_dim.6), calls=%async_computation.1 | async-start | bytes 720896 | tf_op jit(solution)/shard_map/all_to_all | solution.py:53
  321.2 0.3 convert_reduce_fusion
  321.6 1.1 copy.20
  322.7 8.1 %all-to-all-done.1 = bf16[2,128,704]{1,2,0:T(8,128)(2,1)S(1)} async-done(((bf16[2,128,704]{1,2,0:T(8,128)(2,1)}), bf16[2,128,704]{1,2,0:T(8,128)(2,1)S(1)}, u32[]{:S(2)}, u32[]{:S(2)}) %all-to-all-start.1) | async-done | bytes 360480 | tf_op jit(solution)/shard_map/all_to_all | solution.py:53
  330.8 0.8 broadcast_in_dim.7
  331.6 5.0 %all-to-all-start.2 = ((bf16[2,128,704]{1,2,0:T(8,128)(2,1)}), bf16[2,128,704]{1,2,0:T(8,128)(2,1)S(1)}, u32[]{:S(2)}, u32[]{:S(2)}) async-start(bf16[2,128,704]{1,2,0:T(8,128)(2,1)} %broadcast_in_dim.7), calls=%async_computation.2 | async-start | bytes 720896 | tf_op jit(solution)/shard_map/all_to_all | solution.py:53
  336.6 0.2 fusion.26
  336.8 0.2 copy.21
  337.0 9.3 %all-to-all-done.2 = bf16[2,128,704]{1,2,0:T(8,128)(2,1)S(1)} async-done(((bf16[2,128,704]{1,2,0:T(8,128)(2,1)}), bf16[2,128,704]{1,2,0:T(8,128)(2,1)S(1)}, u32[]{:S(2)}, u32[]{:S(2)}) %all-to-all-start.2) | async-done | bytes 360480 | tf_op jit(solution)/shard_map/all_to_all | solution.py:53
  346.2 0.8 broadcast_in_dim.8
  347.0 3.7 %all-to-all-start.3 = ((bf16[2,128,704]{1,2,0:T(8,128)(2,1)}), bf16[2,128,704]{1,2,0:T(8,128)(2,1)S(1)}, u32[]{:S(2)}, u32[]{:S(2)}) async-start(bf16[2,128,704]{1,2,0:T(8,128)(2,1)} %broadcast_in_dim.8), calls=%async_computation.3 | async-start | bytes 720896 | tf_op jit(solution)/shard_map/all_to_all | solution.py:53
  350.7 1.0 fusion.18
  351.7 0.8 convert_reduce_fusion.3
  352.5 0.8 convert_reduce_fusion.2
  353.3 7.1 %all-to-all-done.3 = bf16[2,128,704]{1,2,0:T(8,128)(2,1)S(1)} async-done(((bf16[2,128,704]{1,2,0:T(8,128)(2,1)}), bf16[2,128,704]{1,2,0:T(8,128)(2,1)S(1)}, u32[]{:S(2)}, u32[]{:S(2)}) %all-to-all-start.3) | async-done | bytes 360480 | tf_op jit(solution)/shard_map/all_to_all | solution.py:53
  360.3 0.8 convert_reduce_fusion.1
  (34 shorter events, 0.2 us)
Async XLA Ops:
  7.2 4.6 %copy-start = (bf16[64,2048]{1,0:T(8,128)(2,1)S(1)}, bf16[64,2048]{1,0:T(8,128)(2,1)}, u32[]{:S(2)}) copy-start(bf16[64,2048]{1,0:T(8,128)(2,1)} %param.10) | copy-start | bytes 786436
  7.2 4.6 %copy-start.9 = (f32[2048]{0:T(1024)S(1)}, f32[2048]{0:T(1024)}, u32[]{:S(2)}) copy-start(f32[2048]{0:T(1024)} %param.11) | copy-start | bytes 24580
  7.2 41.4 %all-gather.6.cloned.1.call-start = ((), (), s32[]{:S(2)}) async-start(), calls=%async_computation.6 | async-start | bytes 4718592 | tf_op jit(solution)/shard_map/all_gather | solution.py:24
  9.2 3.6 copy-start.6
  9.2 3.6 copy-start.7
  9.3 3.6 copy-start.8
  12.8 165.1 %all-gather.4.cloned.1.call-start = ((), (), s32[]{:S(2)}) async-start(), calls=%async_computation.5 | async-start | bytes 9191424 | tf_op jit(solution)/shard_map/all_gather | solution.py:12
  13.8 300.4 %reduce-scatter.4.cloned.1.call-start = ((), (), s32[]{:S(2)}) async-start(), calls=%async_computation.7 | async-start | bytes 9469952
  70.0 112.9 %copy-start.3 = (bf16[512,2048]{1,0:T(8,128)(2,1)S(1)}, bf16[512,2048]{1,0:T(8,128)(2,1)}, u32[]{:S(2)}) copy-start(bf16[512,2048]{1,0:T(8,128)(2,1)} %reshape_reshape.7) | copy-start | bytes 6291460
  177.9 5.0 %copy-start.10 = (bf16[512,704]{0,1:T(8,128)(2,1)S(1)}, bf16[512,704]{0,1:T(8,128)(2,1)}, u32[]{:S(2)}) copy-start(bf16[512,704]{0,1:T(8,128)(2,1)} %param.13) | copy-start | bytes 2162692
  182.9 1.8 copy-start.12
  182.9 1.8 copy-start.4
  184.7 1.8 copy-start.1
  202.5 1.1 copy-start.5
  203.6 3.8 %copy-start.11 = (bf16[512,704]{0,1:T(8,128)(2,1)S(1)}, bf16[512,704]{0,1:T(8,128)(2,1)}, u32[]{:S(2)}) copy-start(bf16[512,704]{0,1:T(8,128)(2,1)} %param.13) | copy-start | bytes 2162692
  203.6 3.8 %copy-start.13 = (f32[512,704]{0,1:T(8,128)S(1)}, f32[512,704]{0,1:T(8,128)}, u32[]{:S(2)}) copy-start(f32[512,704]{0,1:T(8,128)} %copy-done.12) | copy-start | bytes 4325380
  212.7 103.5 %all-to-all-start = ((bf16[8,64,2048]{2,1,0:T(8,128)(2,1)}), bf16[8,64,2048]{2,1,0:T(8,128)(2,1)S(1)}, u32[]{:S(2)}, u32[]{:S(2)}) async-start(bf16[8,64,2048]{2,1,0:T(8,128)(2,1)} %bitcast.14), calls=%async_computation | async-start | bytes 4194304 | tf_op jit(solution)/shard_map/all_to_all | solution.py:40
  317.0 13.8 %all-to-all-start.1 = ((bf16[2,128,704]{1,2,0:T(8,128)(2,1)}), bf16[2,128,704]{1,2,0:T(8,128)(2,1)S(1)}, u32[]{:S(2)}, u32[]{:S(2)}) async-start(bf16[2,128,704]{1,2,0:T(8,128)(2,1)} %broadcast_in_dim.6), calls=%async_computation.1 | async-start | bytes 720896 | tf_op jit(solution)/shard_map/all_to_all | solution.py:53
  321.6 29.1 %copy-start.2 = (bf16[64,2048]{1,0:T(8,128)(2,1)S(1)}, bf16[64,2048]{1,0:T(8,128)(2,1)}, u32[]{:S(2)}) copy-start(bf16[64,2048]{1,0:T(8,128)(2,1)} %param.16) | copy-start | bytes 786436
  331.6 14.6 %all-to-all-start.2 = ((bf16[2,128,704]{1,2,0:T(8,128)(2,1)}), bf16[2,128,704]{1,2,0:T(8,128)(2,1)S(1)}, u32[]{:S(2)}, u32[]{:S(2)}) async-start(bf16[2,128,704]{1,2,0:T(8,128)(2,1)} %broadcast_in_dim.7), calls=%async_computation.2 | async-start | bytes 720896 | tf_op jit(solution)/shard_map/all_to_all | solution.py:53
  347.0 13.3 %all-to-all-start.3 = ((bf16[2,128,704]{1,2,0:T(8,128)(2,1)}), bf16[2,128,704]{1,2,0:T(8,128)(2,1)S(1)}, u32[]{:S(2)}, u32[]{:S(2)}) async-start(bf16[2,128,704]{1,2,0:T(8,128)(2,1)} %broadcast_in_dim.8), calls=%async_computation.3 | async-start | bytes 720896 | tf_op jit(solution)/shard_map/all_to_all | solution.py:53
Sparse Core Ops, SparseCore 0:
  12.9 35.6 all-gather.5
  50.3 127.5 all-gather.3
  202.6 111.4 reduce-scatter.3
where the time goes:
time: 371 us; the launch traced here: 368 us
  waiting for transfers between devices  264 us (71%)
  local copies, waits for them, and re-layouts  34.6 us (9%)
  matrix products  22.9 us (6%)
  starting transfers between devices  17.9 us (5%)
  other arithmetic  14.4 us (4%)
  between operations  14 us (4%)
    all_gather x1, waiting for transfers between devices, side_by_side(): whole = lax.all_gather(both, axis, axis=dim, tiled=True)  108 us
    unnamed x4, waiting for transfers between devices  96.7 us
    all_gather x1, waiting for transfers between devices, gather_together(): lines, at, finished = (lax.all_gather(flat, axis), 0, [])  34.8 us
    all_to_all x3, waiting for transfers between devices, copy_for_each(): lax.all_to_all(jnp.broadcast_to(shard[None], (size, *shard.shape)), axis,...  24.4 us
    unnamed x34, local copies, waits for them, and re-layouts  14.4 us
    all_to_all x3, starting transfers between devices, copy_for_each(): lax.all_to_all(jnp.broadcast_to(shard[None], (size, *shard.shape)), axis,...  13 us
    dot_general x2, matrix products, contract_cols(): lax.dot_general(left, right, (((1,), (1,)), ((), ())), preferred_element_...  9.08 us
    dot_general x3, matrix products, contract_rows(): lax.dot_general(left, right, (((0,), (0,)), ((), ())), preferred_element_...  8.89 us
  transfers between devices with their start and end apart: 7, of which 6 were waited for; matrix products, arithmetic and copies ran while one was open for 10% of the time, Pallas kernels for 0%

commit v1 on v0

v1 whole, which is shorter than its diff:
```python
import jax
import jax.numpy as jnp
from jax import lax
from jax.experimental import pallas as pl
from jax.experimental.pallas import tpu as pltpu
from jax.sharding import PartitionSpec as P

MESH = pl.DeviceIdType.MESH
bf16, f32 = jnp.bfloat16, jnp.float32
eps = 1e-06

H = 704
A, B = (0, 352), (352, 352)
QA, QB = ((0, 176), (176, 176)), ((352, 176), (528, 176))
P0, P1 = (0, 256), (256, 256)
Q0, Q1 = (0, 96), (96, 96)
QS = 512
N_SEM = 224


def ds(r):
    return pl.ds(r[0], r[1])


def mod(a, n):
    return lax.rem(a + n, n)


def kernel(
    x_ref, pre_ref, post_ref, gs_ref, us_ref, br_ref, oc_ref, gw_ref, uw_ref, dw_ref,
    ig_ref, gg_ref, ug_ref, dg_ref,
    W, R, G, RY1, RYa, RYb, RZ1, RZa, RZb, SY1, SYa, SYb, SZ1, SZa, SZb,
    T, XF, XR, silu, dgate, hid, cot, cotT, NG, NS, NX1, NXa, NXb, ssem, rsem,
):
    rep, fs, tp = lax.axis_index("rep"), lax.axis_index("fs"), lax.axis_index("tp")
    zl, y = fs // 4, fs % 4
    z = rep * 4 + zl
    x, core = tp // 2, tp % 2
    ym, yp, y2 = mod(y - 1, 4), mod(y + 1, 4), mod(y + 2, 4)
    zm, zp, z2 = mod(zl - 1, 4), mod(zl + 1, 4), mod(zl + 2, 4)
    xm, xp, x2 = mod(x - 1, 4), mod(x + 1, 4), mod(x + 2, 4)

    def zdev(d):
        zz = mod(z + d, 8)
        return {"rep": zz // 4, "fs": (zz % 4) * 4 + y}

    dev = {
        "y+": {"fs": zl * 4 + yp},
        "y-": {"fs": zl * 4 + ym},
        "z+": zdev(1),
        "z-": zdev(-1),
        "zz+": zdev(2),
        "zz-": zdev(-2),
        "x+": {"tp": xp * 2 + core},
        "x-": {"tp": xm * 2 + core},
        "s": {"tp": x * 2 + 1 - core},
    }

    barrier = pltpu.get_barrier_semaphore()
    for name in dev:
        pl.semaphore_signal(barrier, inc=1, device_id=dev[name], device_id_type=MESH)

    ids = {}
    sends = []

    def number(key):
        return ids.setdefault(key, len(ids))

    def send(key, src, dst, to):
        k = number(key)
        c = pltpu.make_async_remote_copy(
            src_ref=src, dst_ref=dst, send_sem=ssem.at[k], recv_sem=rsem.at[k],
            device_id=dev[to], device_id_type=MESH,
        )
        c.start()
        sends.append(c)

    def recv(key, ref, frm):
        k = number(key)
        pltpu.make_async_remote_copy(
            src_ref=ref, dst_ref=ref, send_sem=ssem.at[k], recv_sem=rsem.at[k],
            device_id=dev[frm], device_id_type=MESH,
        ).wait_recv()

    xf = x_ref[...].astype(f32)
    inv_x = lax.rsqrt(jnp.mean(xf * xf, axis=-1, keepdims=True) + eps)
    R[0, tp] = (xf * inv_x * pre_ref[...]).astype(bf16)
    br = br_ref[...].astype(f32)
    inv_b = lax.rsqrt(jnp.mean(br * br, axis=-1, keepdims=True) + eps)
    upst = 0.5 * oc_ref[...].astype(f32) * post_ref[...]
    R[1, tp] = (
        inv_b * upst - br * (inv_b * inv_b * inv_b) * jnp.mean(upst * br, axis=-1, keepdims=True)
    ).astype(bf16)
    own = (dw_ref, gw_ref, uw_ref)
    for m in range(3):
        W[m, zl, y] = own[m][...]

    pl.semaphore_wait(barrier, len(dev))

    def ag_own(m):
        for to in ("y+", "y-", "z+", "z-"):
            send(("o", m, to), own[m], W.at[m, zl, y], to)

    def ag_near(m):
        s = W.at[m, zl, ym]
        recv(("o", m, "y+"), s, "y-")
        a = W.at[m, zl, ym, ds(A)]
        send(("f", m, "y+"), a, a, "y+")
        for to in ("z+", "z-"):
            send(("d", m, 0, to), a, a, to)
        s = W.at[m, zl, yp]
        recv(("o", m, "y-"), s, "y+")
        b = W.at[m, zl, yp, ds(B)]
        send(("f", m, "y-"), b, b, "y-")
        a = W.at[m, zl, yp, ds(A)]
        for to in ("z+", "z-"):
            send(("d", m, 1, to), a, a, to)
        s = W.at[m, zm, y]
        recv(("o", m, "z+"), s, "z-")
        a = W.at[m, zm, y, ds(A)]
        send(("f", m, "z+"), a, a, "z+")
        b = W.at[m, zm, y, ds(B)]
        for to in ("y+", "y-"):
            send(("d", m, 0, to), b, b, to)
        s = W.at[m, zp, y]
        recv(("o", m, "z-"), s, "z+")
        b = W.at[m, zp, y, ds(B)]
        send(("f", m, "z-"), b, b, "z-")
        for to in ("y+", "y-"):
            send(("d", m, 1, to), b, b, to)

    def ag_mid(m):
        a = W.at[m, zl, y2, ds(A)]
        recv(("f", m, "y+"), a, "y-")
        for to in ("z+", "z-"):
            send(("d", m, 2, to), a, a, to)
        b = W.at[m, z2, y, ds(B)]
        recv(("f", m, "z-"), b, "z+")
        for to in ("y+", "y-"):
            send(("d", m, 2, to), b, b, to)

    def ag_diag(m, k):
        yk, zk = (ym, yp, y2)[k], (zm, zp, z2)[k]
        for frm, to, slot, q, part in (
            ("z-", "z+", (zm, yk), QA[0], A),
            ("z+", "z-", (zp, yk), QA[1], A),
            ("y-", "y+", (zk, ym), QB[0], B),
            ("y+", "y-", (zk, yp), QB[1], B),
        ):
            recv(("d", m, k, to), W.at[m, slot[0], slot[1], ds(part)], frm)
            r = W.at[m, slot[0], slot[1], ds(q)]
            send(("e", m, k, to), r, r, to)

    def ag_end(m):
        b = W.at[m, zl, y2, ds(B)]
        recv(("f", m, "y-"), b, "y+")
        a = W.at[m, z2, y, ds(A)]
        recv(("f", m, "z+"), a, "z-")
        for k in range(3):
            yk, zk = (ym, yp, y2)[k], (zm, zp, z2)[k]
            recv(("e", m, k, "z+"), W.at[m, z2, yk, ds(QA[0])], "z-")
            recv(("e", m, k, "z-"), W.at[m, z2, yk, ds(QA[1])], "z+")
            recv(("e", m, k, "y+"), W.at[m, zk, y2, ds(QB[0])], "y-")
            recv(("e", m, k, "y-"), W.at[m, zk, y2, ds(QB[1])], "y+")

    sib = 1 - core
    C = (pl.ds(0, 1024), pl.ds(1024, 1024))

    def rows_own(n):
        r = R.at[n, tp]
        for to in ("x+", "x-", "s"):
            send(("r", n, to), r, r, to)

    def rows_near(n):
        for frm, to, slot, c in (
            ("x-", "x+", xm * 2 + core, C[0]),
            ("x+", "x-", xp * 2 + core, C[1]),
        ):
            r = R.at[n, slot]
            recv(("r", n, to), r, frm)
            q = R.at[n, slot, :, c]
            send(("rf", n, to), q, q, to)
            send(("rs", n, frm), r, r, "s")

    def rows_far(n):
        slot = x2 * 2 + core
        recv(("rf", n, "x+"), R.at[n, slot, :, C[0]], "x-")
        recv(("rf", n, "x-"), R.at[n, slot, :, C[1]], "x+")
        r = R.at[n, slot]
        send(("rs", n, "2"), r, r, "s")

    def rows_end(n):
        recv(("r", n, "s"), R.at[n, x * 2 + sib], "s")
        recv(("rs", n, "x-"), R.at[n, xm * 2 + sib], "s")
        recv(("rs", n, "x+"), R.at[n, xp * 2 + sib], "s")
        recv(("rs", n, "2"), R.at[n, x2 * 2 + sib], "s")

    def factors():
        def body(i, _):
            r = pl.ds(pl.multiple_of(i * 32, 32), 32)
            g, u = gs_ref[r, :].astype(f32), us_ref[r, :].astype(f32)
            s = jax.nn.sigmoid(g)
            v = g * s
            silu[r, :] = v
            hid[r, :] = (v * u).astype(bf16)
            dgate[r, :] = u * s * (1.0 + g * (1.0 - s))
            return 0

        lax.fori_loop(0, H // 32, body, 0)

    def partial(m, left, off, n):
        def body(c, _):
            cols = pl.ds(pl.multiple_of(c * 256, 256), 256)
            right = R[n, :, :, cols].reshape(512, 256)
            out = jnp.dot(left[off : off + H, :], right, preferred_element_type=f32).astype(bf16)
            G[m, c // 2, (c % 2) * 2] = out[:, :128]
            G[m, c // 2, (c % 2) * 2 + 1] = out[:, 128:]
            return 0

        lax.fori_loop(0, 8, body, 0)

    def hidden_grad():
        def body(t, _):
            right = R[1, pl.ds(t * 4, 4)].reshape(256, 2048)
            left = jnp.concatenate([W[0, k // 4, k % 4] for k in range(16)], axis=1)
            hg = lax.dot_general(
                left, right, (((1,), (1,)), ((), ())), preferred_element_type=f32
            )
            cols = pl.ds(pl.multiple_of(t * 256, 256), 256)
            cot[pl.ds(0, H), cols] = (hg * dgate[:, cols]).astype(bf16)
            cot[pl.ds(H, H), cols] = (hg * silu[:, cols]).astype(bf16)
            return 0

        lax.fori_loop(0, 2, body, 0)

    def turn():
        for k in range(11):
            cotT[:, k * 128 : (k + 1) * 128] = cot[k * 128 : (k + 1) * 128, :].T

    def normed_grad():
        def body(c, _):
            left = cotT[...]
            zz, yy = c // 2, (c % 2) * 2
            right = jnp.concatenate(
                [
                    jnp.concatenate([W[1, zz, yy + k], W[2, zz, yy + k]], axis=0)
                    for k in range(2)
                ],
                axis=1,
            )
            out = jnp.dot(left, right, preferred_element_type=f32).astype(bf16)
            cols = pl.ds(pl.multiple_of(c * 256, 256), 256)
            NG[:, :, :, cols] = out.reshape(4, 2, 64, 256)
            return 0

        lax.fori_loop(0, 8, body, 0)

    def ng_pair():
        send("np", NG.at[:, sib], NS, "s")

    def ng_first():
        recv("np", NS, "s")

        for k in range(4):
            NG[k, core] = NG[k, core] + NS[k]
        send("n1+", NG.at[x2, core, :, C[0]], NX1.at[0], "x+")
        send("n1-", NG.at[x2, core, :, C[1]], NX1.at[1], "x-")
        send("na+", NG.at[xp, core, :, C[1]], NXa.at[0], "x+")
        send("na-", NG.at[xm, core, :, C[0]], NXa.at[1], "x-")

    def ng_second():
        recv("n1+", NX1.at[0], "x-")
        NG[xp, core, :, C[0]] = NG[xp, core, :, C[0]] + NX1[0]
        send("nb+", NG.at[xp, core, :, C[0]], NXb.at[0], "x+")
        recv("n1-", NX1.at[1], "x+")
        NG[xm, core, :, C[1]] = NG[xm, core, :, C[1]] + NX1[1]
        send("nb-", NG.at[xm, core, :, C[1]], NXb.at[1], "x-")

    def ng_end():
        recv("na+", NXa.at[0], "x-")
        recv("na-", NXa.at[1], "x+")
        recv("nb+", NXb.at[0], "x-")
        recv("nb-", NXb.at[1], "x+")
        mine = NG[x, core].astype(f32)
        h0 = mine[:, :1024] + NXb[0].astype(f32) + NXa[1].astype(f32)
        h1 = mine[:, 1024:] + NXb[1].astype(f32) + NXa[0].astype(f32)
        w = jnp.concatenate([h0, h1], axis=1) * pre_ref[...]
        xv = x_ref[...].astype(f32)
        inv = lax.rsqrt(jnp.mean(xv * xv, axis=-1, keepdims=True) + eps)
        ig_ref[...] = (
            oc_ref[...].astype(f32)
            + inv * w
            - xv * (inv * inv * inv) * jnp.mean(w * xv, axis=-1, keepdims=True)
        ).astype(bf16)

    def q(r):
        return pl.ds(QS + r[0], r[1])

    def rs_first(m):
        g = G.at[m]
        send(("a1", m, "y+"), g.at[:, y2, ds(P0)], RY1.at[m, 0], "y+")
        send(("a1", m, "y-"), g.at[:, y2, ds(P1)], RY1.at[m, 1], "y-")
        send(("b1", m, "z+"), g.at[z2, :, q(Q0)], RZ1.at[m, 0], "z+")
        send(("b1", m, "z-"), g.at[z2, :, q(Q1)], RZ1.at[m, 1], "z-")
        send(("aa", m, "y+"), g.at[:, yp, ds(P1)], RYa.at[m, 0], "y+")
        send(("aa", m, "y-"), g.at[:, ym, ds(P0)], RYa.at[m, 1], "y-")
        send(("ba", m, "z+"), g.at[zp, :, q(Q1)], RZa.at[m, 0], "z+")
        send(("ba", m, "z-"), g.at[zm, :, q(Q0)], RZa.at[m, 1], "z-")

    def rs_second(m):
        g = G.at[m]
        recv(("b1", m, "z+"), RZ1.at[m, 0], "z-")
        G[m, zp, :, q(Q0)] = G[m, zp, :, q(Q0)] + RZ1[m, 0]
        send(("bb", m, "z+"), g.at[zp, :, q(Q0)], RZb.at[m, 0], "z+")
        recv(("b1", m, "z-"), RZ1.at[m, 1], "z+")
        G[m, zm, :, q(Q1)] = G[m, zm, :, q(Q1)] + RZ1[m, 1]
        send(("bb", m, "z-"), g.at[zm, :, q(Q1)], RZb.at[m, 1], "z-")
        recv(("a1", m, "y+"), RY1.at[m, 0], "y-")
        G[m, :, yp, ds(P0)] = G[m, :, yp, ds(P0)] + RY1[m, 0]
        send(("ab", m, "y+"), g.at[:, yp, ds(P0)], RYb.at[m, 0], "y+")
        recv(("a1", m, "y-"), RY1.at[m, 1], "y+")
        G[m, :, ym, ds(P1)] = G[m, :, ym, ds(P1)] + RY1[m, 1]
        send(("ab", m, "y-"), g.at[:, ym, ds(P1)], RYb.at[m, 1], "y-")

    def add3(a, b, c):
        return (a.astype(f32) + b.astype(f32) + c.astype(f32)).astype(bf16)

    def rs_third(m):
        g = G.at[m]
        recv(("ba", m, "z+"), RZa.at[m, 0], "z-")
        recv(("ba", m, "z-"), RZa.at[m, 1], "z+")
        recv(("bb", m, "z+"), RZb.at[m, 0], "z-")
        recv(("bb", m, "z-"), RZb.at[m, 1], "z+")
        G[m, zl, :, q(Q0)] = add3(G[m, zl, :, q(Q0)], RZb[m, 0], RZa[m, 1])
        G[m, zl, :, q(Q1)] = add3(G[m, zl, :, q(Q1)], RZb[m, 1], RZa[m, 0])
        send(("c1", m, "y+"), g.at[zl, y2, q(Q0)], SY1.at[m, 0], "y+")
        send(("c1", m, "y-"), g.at[zl, y2, q(Q1)], SY1.at[m, 1], "y-")
        send(("ca", m, "y+"), g.at[zl, yp, q(Q1)], SYa.at[m, 0], "y+")
        send(("ca", m, "y-"), g.at[zl, ym, q(Q0)], SYa.at[m, 1], "y-")
        recv(("aa", m, "y+"), RYa.at[m, 0], "y-")
        recv(("aa", m, "y-"), RYa.at[m, 1], "y+")
        recv(("ab", m, "y+"), RYb.at[m, 0], "y-")
        recv(("ab", m, "y-"), RYb.at[m, 1], "y+")
        G[m, :, y, ds(P0)] = add3(G[m, :, y, ds(P0)], RYb[m, 0], RYa[m, 1])
        G[m, :, y, ds(P1)] = add3(G[m, :, y, ds(P1)], RYb[m, 1], RYa[m, 0])
        send(("d1", m, "z+"), g.at[z2, y, ds(P0)], SZ1.at[m, 0], "z+")
        send(("d1", m, "z-"), g.at[z2, y, ds(P1)], SZ1.at[m, 1], "z-")
        send(("da", m, "z+"), g.at[zp, y, ds(P1)], SZa.at[m, 0], "z+")
        send(("da", m, "z-"), g.at[zm, y, ds(P0)], SZa.at[m, 1], "z-")

    def rs_fourth(m):
        g = G.at[m]
        recv(("c1", m, "y+"), SY1.at[m, 0], "y-")
        G[m, zl, yp, q(Q0)] = G[m, zl, yp, q(Q0)] + SY1[m, 0]
        send(("cb", m, "y+"), g.at[zl, yp, q(Q0)], SYb.at[m, 0], "y+")
        recv(("c1", m, "y-"), SY1.at[m, 1], "y+")
        G[m, zl, ym, q(Q1)] = G[m, zl, ym, q(Q1)] + SY1[m, 1]
        send(("cb", m, "y-"), g.at[zl, ym, q(Q1)], SYb.at[m, 1], "y-")
        recv(("d1", m, "z+"), SZ1.at[m, 0], "z-")
        G[m, zp, y, ds(P0)] = G[m, zp, y, ds(P0)] + SZ1[m, 0]
        send(("db", m, "z+"), g.at[zp, y, ds(P0)], SZb.at[m, 0], "z+")
        recv(("d1", m, "z-"), SZ1.at[m, 1], "z+")
        G[m, zm, y, ds(P1)] = G[m, zm, y, ds(P1)] + SZ1[m, 1]
        send(("db", m, "z-"), g.at[zm, y, ds(P1)], SZb.at[m, 1], "z-")

    X0, X1 = pl.ds(0, 352), pl.ds(352, 352)

    def rs_fifth(m):
        recv(("ca", m, "y+"), SYa.at[m, 0], "y-")
        recv(("ca", m, "y-"), SYa.at[m, 1], "y+")
        recv(("cb", m, "y+"), SYb.at[m, 0], "y-")
        recv(("cb", m, "y-"), SYb.at[m, 1], "y+")
        T[m, q(Q0)] = add3(G[m, zl, y, q(Q0)], SYb[m, 0], SYa[m, 1])
        T[m, q(Q1)] = add3(G[m, zl, y, q(Q1)], SYb[m, 1], SYa[m, 0])
        recv(("da", m, "z+"), SZa.at[m, 0], "z-")
        recv(("da", m, "z-"), SZa.at[m, 1], "z+")
        recv(("db", m, "z+"), SZb.at[m, 0], "z-")
        recv(("db", m, "z-"), SZb.at[m, 1], "z+")
        T[m, ds(P0)] = add3(G[m, zl, y, ds(P0)], SZb[m, 0], SZa[m, 1])
        T[m, ds(P1)] = add3(G[m, zl, y, ds(P1)], SZb[m, 1], SZa[m, 0])
        send(("x", m, "zz+"), T.at[m, X0], XF.at[m, 0], "zz+")
        send(("x", m, "zz-"), T.at[m, X1], XF.at[m, 1], "zz-")

    def rs_sixth(m):
        recv(("x", m, "zz+"), XF.at[m, 0], "zz-")
        send(("xf", m, "zz+"), XF.at[m, 0], XR.at[m, X0], "zz+")
        recv(("x", m, "zz-"), XF.at[m, 1], "zz+")
        send(("xf", m, "zz-"), XF.at[m, 1], XR.at[m, X1], "zz-")

    outs = (dg_ref, gg_ref, ug_ref)

    def rs_end(m):
        recv(("xf", m, "zz+"), XR.at[m, X0], "zz-")
        recv(("xf", m, "zz-"), XR.at[m, X1], "zz+")
        outs[m][...] = T[m].astype(f32) + XR[m].astype(f32)

    ag_own(0)
    rows_own(1)
    rows_own(0)
    ag_own(1)
    factors()
    ag_near(0)
    ag_own(2)
    rows_near(1)
    ag_near(1)
    rows_near(0)
    ag_mid(0)
    ag_near(2)
    ag_diag(0, 0)
    ag_diag(0, 1)
    rows_far(1)
    ag_mid(1)
    rows_far(0)
    ag_diag(0, 2)
    rows_end(1)
    partial(0, hid, 0, 1)
    rs_first(0)
    ag_mid(2)
    ag_diag(1, 0)
    ag_diag(1, 1)
    ag_end(0)
    hidden_grad()
    rows_end(0)
    partial(1, cot, 0, 0)
    rs_first(1)
    ag_diag(1, 2)
    ag_diag(2, 0)
    ag_diag(2, 1)
    partial(2, cot, H, 0)
    rs_first(2)
    ag_diag(2, 2)
    rs_second(0)
    turn()
    ag_end(1)
    ag_end(2)
    normed_grad()
    ng_pair()
    rs_third(0)
    rs_second(1)
    ng_first()
    rs_fourth(0)
    ng_second()
    rs_second(2)
    rs_third(1)
    rs_fifth(0)
    rs_fourth(1)
    ng_end()
    rs_sixth(0)
    rs_third(2)
    rs_fifth(1)
    rs_fourth(2)
    rs_sixth(1)
    rs_end(0)
    rs_fifth(2)
    rs_end(1)
    rs_sixth(2)
    rs_end(2)
    for c in sends:
        c.wait_send()


def per_device(x, pre, post, gs, us, br, oc, gw, uw, dw):
    vmem = pl.BlockSpec(memory_space=pltpu.VMEM)
    V = pltpu.VMEM
    sds = jax.ShapeDtypeStruct
    ig, gg, ug, dg = pl.pallas_call(
        kernel,
        out_shape=(
            sds((64, 2048), bf16), sds((H, 128), f32), sds((H, 128), f32), sds((H, 128), f32),
        ),
        in_specs=[vmem] * 10,
        out_specs=(vmem,) * 4,
        scratch_shapes=[
            V((3, 4, 4, H, 128), bf16),
            V((2, 8, 64, 2048), bf16),
            V((3, 4, 4, H, 128), bf16),
            V((3, 2, 4, 256, 128), bf16),
            V((3, 2, 4, 256, 128), bf16),
            V((3, 2, 4, 256, 128), bf16),
            V((3, 2, 4, 96, 128), bf16),
            V((3, 2, 4, 96, 128), bf16),
            V((3, 2, 4, 96, 128), bf16),
            V((3, 2, 96, 128), bf16),
            V((3, 2, 96, 128), bf16),
            V((3, 2, 96, 128), bf16),
            V((3, 2, 256, 128), bf16),
            V((3, 2, 256, 128), bf16),
            V((3, 2, 256, 128), bf16),
            V((3, H, 128), bf16),
            V((3, 2, 352, 128), bf16),
            V((3, H, 128), bf16),
            V((H, 512), f32),
            V((H, 512), f32),
            V((H, 512), bf16),
            V((2 * H, 512), bf16),
            V((512, 2 * H), bf16),
            V((4, 2, 64, 2048), bf16),
            V((4, 64, 2048), bf16),
            V((2, 64, 1024), bf16),
            V((2, 64, 1024), bf16),
            V((2, 64, 1024), bf16),
            pltpu.SemaphoreType.DMA((N_SEM,)),
            pltpu.SemaphoreType.DMA((N_SEM,)),
        ],
        compiler_params=pltpu.CompilerParams(
            collective_id=0, has_side_effects=True, vmem_limit_bytes=66 * 1000 * 1000
        ),
        name="ffn_backward",
    )(x, pre.reshape(1, -1), post.reshape(1, -1), gs.T, us.T, br, oc, gw.T, uw.T, dw.T)
    return ig, gg.T, ug.T, dg.T


def solution(mesh):
    return jax.shard_map(
        per_device,
        mesh=mesh,
        in_specs=(
            P(("rep", "fs", "tp"), None),
            P(),
            P(),
            P(("rep", "fs"), "tp"),
            P(("rep", "fs"), "tp"),
            P(("rep", "fs", "tp"), None),
            P(("rep", "fs", "tp"), None),
            P("fs", "tp"),
            P("fs", "tp"),
            P("fs", "tp"),
        ),
        out_specs=(P(("rep", "fs", "tp"), None), P("fs", "tp"), P("fs", "tp"), P("fs", "tp")),
        check_vma=False,
    )
```

time: 371 us -> 152 us (0.41)
  waiting for transfers between devices: 264 us -> 0 us
  Pallas kernels: 0 us -> 146 us
  local copies, waits for them, and re-layouts: 34.6 us -> 4.69 us
  matrix products: 22.9 us -> 0 us
  starting transfers between devices: 17.9 us -> 0 us
  other arithmetic: 14.4 us -> 0 us
  between operations: 14 us -> 0.65 us
    pallas_call x0 -> x1, Pallas kernels: none -> 146 us  [per_device(): pl.pallas_call(kernel, out_shape=(sds((64, 2048), bf16), sds((H, 128), f3...]
    all_gather x2 -> x0, waiting for transfers between devices: 143 us -> none  [the longest x1 108 us: side_by_side(): whole = lax.all_gather(both, axis, axis=dim, tiled=True)]
    unnamed x4 -> x0, waiting for transfers between devices: 96.7 us -> none
    all_to_all x4 -> x0, waiting for transfers between devices: 24.4 us -> none  [the longest x3 24.4 us: copy_for_each(): lax.all_to_all(jnp.broadcast_to(shard[None], (size, *shard.shape)), axis,...]
    dot_general x6 -> x0, matrix products: 22.9 us -> none  [the longest x2 9.08 us: contract_cols(): lax.dot_general(left, right, (((1,), (1,)), ((), ())), preferred_element_...]
    all_to_all x4 -> x0, starting transfers between devices: 17.8 us -> none  [the longest x3 13 us: copy_for_each(): lax.all_to_all(jnp.broadcast_to(shard[None], (size, *shard.shape)), axis,...]
    unnamed x34 -> x10, local copies, waits for them, and re-layouts: 14.4 us -> 4.69 us
    another operation x2 -> x0, local copies, waits for them, and re-layouts: 6.2 us -> none  [joined_along(): return jnp.moveaxis(blocks, 0, dim).reshape(lengths)]
  transfers between devices with their start and end apart: 7 -> 0, of which waited for: 6 -> 0; matrix products, arithmetic and copies ran while one was open for 10% -> 0% of each run, Pallas kernels for 0% -> 0%
where the time goes in v1:
time: 152 us; the launch traced here: 151 us
  Pallas kernels  146 us (96%)
  local copies, waits for them, and re-layouts  4.69 us (3%)
    pallas_call x1, Pallas kernels, per_device(): pl.pallas_call(kernel, out_shape=(sds((64, 2048), bf16), sds((H, 128), f3...  146 us
    unnamed x10, local copies, waits for them, and re-layouts  4.69 us

profile of v1, /device:TPU:6, one launch (start us, length us, event | category | flops | bytes accessed | tf_op | source)
XLA Modules:
  0.0 151.1 jit_solution(6279167540597177882)
XLA Ops:
  0.6 145.7 %ffn_backward.1 = (bf16[64,2048]{1,0:T(8,128)(2,1)}, f32[704,128]{1,0:T(8,128)}, f32[704,128]{1,0:T(8,128)}, f32[704,128]{1,0:T(8,128)}) custom-call(bf16[64,2048]{1,0:T(8,128)(2,1)} %x_ref.1, f32[1,2048]{1,0:T(1,128)} %bitcast.18, f32[1,2048]{1,0:T(1,128)} %bitcast.19, bf16[704,512]{1,0:T(8,128)(2,1)} %bitcast.10, bf16[704,512]{1,0:T(8,128)(2,1)} %bitcast.11, ...), custom_call_target="tpu_custom_call" | custom-call | tf_op jit(solution)/shard_map/ffn_backward/pallas_call | solution.py:466
  146.4 0.0 copy-start.2
  146.4 1.7 %copy.18 = bf16[64,2048]{1,0:T(8,128)(2,1)} copy(bf16[64,2048]{1,0:T(8,128)(2,1)} %get-tuple-element.16) | data formatting | bytes 524288
  148.1 0.0 copy-done.2
  148.1 0.0 copy-start.1
  148.1 0.7 copy.19
  148.8 0.4 copy-done.1
  149.2 0.0 copy-start
  149.2 0.7 copy.20
  150.0 0.4 copy-done
  150.3 0.7 copy.21
Async XLA Ops:
  146.4 1.7 %copy-start.2 = (f32[704,128]{1,0:T(8,128)S(1)}, f32[704,128]{1,0:T(8,128)}, u32[]{:S(2)}) copy-start(f32[704,128]{1,0:T(8,128)} %get-tuple-element.9) | copy-start | bytes 1081348
  148.1 1.1 copy-start.1
  149.2 1.1 copy-start

commit v2 on v0

v2 whole, which is shorter than its diff:
```python
import jax
import jax.numpy as jnp
from jax import lax
from jax.experimental import pallas as pl
from jax.experimental.pallas import tpu as pltpu
from jax.sharding import PartitionSpec as P

MESH = pl.DeviceIdType.MESH
bf16, f32 = jnp.bfloat16, jnp.float32
eps = 1e-06

H = 704
NA = (576, 32, 416)
NP = (384, 416, 448)
N_RECV, N_SEND, N_LOCAL = 160, 48, 32
ORDER = (
    2, 51, 3, 85, 27, 0, 80, 1, 75, 81, 82, 19, 9, 10, 4, 5, 14, 15, 20, 33, 43, 38, 28, 76, 77, 25,
    11, 12, 57, 58, 62, 52, 53, 67, 68, 63, 24, 17, 83, 6, 22, 7, 84, 86, 78, 8, 99, 21, 98, 16, 13,
    72, 79, 55, 60, 54, 65, 59, 70, 102, 103, 105, 106, 108, 69, 109, 111, 44, 39, 29, 34, 49, 48,
    112, 64, 73, 18, 23, 101, 104, 113, 120, 107, 36, 31, 66, 71, 35, 40, 30, 41, 42, 45, 46, 47,
    37, 26, 87, 122, 110, 32, 115, 88, 61, 129, 56, 89, 158, 100, 90, 159, 116, 50, 123, 74, 91,
    163, 162, 92, 166, 168, 93, 169, 165, 171, 172, 95, 173, 180, 94, 114, 121, 96, 161, 128, 117,
    124, 164, 167, 160, 170, 175, 118, 182, 125, 97, 132, 143, 150, 133, 135, 136, 138, 139, 176,
    141, 183, 142, 119, 126, 130, 174, 181, 131, 177, 184, 134, 137, 127, 140, 145, 152, 144, 151,
    178, 185, 148, 155, 146, 153, 179, 186, 149, 156, 147, 154, 187, 157,
)


def halves(lo, hi):
    n = (hi - lo) // 2
    return (lo, hi - lo), (lo, n), (lo + n, n)


GA = [halves(0, n) for n in NA]
GB = [halves(n, H) for n in NA]
SP = [halves(0, n) for n in NP]
SQ = [halves(n, H) for n in NP]


def ds(r):
    return pl.ds(r[0], r[1])


def mod(a, n):
    return lax.rem(a + n, n)


def kernel(
    x_hbm, pre_hbm, post_hbm, gs_hbm, us_hbm, br_hbm, oc_hbm, gw_ref, uw_ref, dw_ref,
    ig_hbm, d_my, g_my, u_my, d_th, g_th, u_th,
    *scratch,
):
    s = dict(zip(SCRATCH, scratch))
    W, R, G, T, XF = s["W"], s["R"], s["G"], s["T"], s["XF"]
    silu, dgate, hid, cot, cotT = s["silu"], s["dgate"], s["hid"], s["cot"], s["cotT"]
    NG, NS, NX1, NXc = s["NG"], s["NS"], s["NX1"], s["NXc"]
    x_ref, pre_ref, post_ref, br_ref, oc_ref = s["x"], s["pre"], s["post"], s["br"], s["oc"]
    gs_ref, us_ref, ig_ref = s["gs"], s["us"], s["ig"]
    mine, theirs = (d_my, g_my, u_my), (d_th, g_th, u_th)
    ssem, rsem, lsem = s["ssem"], s["rsem"], s["lsem"]
    RY1, RYc, RZ1, RZc, SY1, SYc, SZ1, SZc = (
        [s[n + k + str(m)] for m in range(3)] for n in ("RY", "RZ", "SY", "SZ") for k in "1c"
    )
    rep, fs, tp = lax.axis_index("rep"), lax.axis_index("fs"), lax.axis_index("tp")
    zl, y = fs // 4, fs % 4
    z = rep * 4 + zl
    x, core = tp // 2, tp % 2
    ym, yp, y2 = mod(y - 1, 4), mod(y + 1, 4), mod(y + 2, 4)
    zm, zp, z2 = mod(zl - 1, 4), mod(zl + 1, 4), mod(zl + 2, 4)
    xm, xp, x2 = mod(x - 1, 4), mod(x + 1, 4), mod(x + 2, 4)

    def zdev(d):
        zz = mod(z + d, 8)
        return {"rep": zz // 4, "fs": (zz % 4) * 4 + y}

    dev = {
        "y+": {"fs": zl * 4 + yp},
        "y-": {"fs": zl * 4 + ym},
        "z+": zdev(1),
        "z-": zdev(-1),
        "zz+": zdev(2),
        "zz-": zdev(-2),
        "x+": {"tp": xp * 2 + core},
        "x-": {"tp": xm * 2 + core},
        "s": {"tp": x * 2 + 1 - core},
    }

    barrier = pltpu.get_barrier_semaphore()
    for name in dev:
        pl.semaphore_signal(barrier, inc=1, device_id=dev[name], device_id_type=MESH)

    ids = {}
    sends = []
    count = [0]

    def number(key):
        return ids.setdefault(key, len(ids))

    def send(key, src, dst, to):
        if 0 in src.shape:
            return
        if len(sends) == N_SEND:
            sends.pop(0).wait_send()
        c = pltpu.make_async_remote_copy(
            src_ref=src, dst_ref=dst, send_sem=ssem.at[count[0] % N_SEND],
            recv_sem=rsem.at[number(key)], device_id=dev[to], device_id_type=MESH,
        )
        c.start()
        count[0] += 1
        sends.append(c)

    def recv(key, ref):
        if 0 in ref.shape:
            return
        k = number(key)
        pltpu.make_async_copy(ref, ref, rsem.at[k]).wait()

    own = (dw_ref, gw_ref, uw_ref)
    local = {}

    def load(key, src, dst):
        c = pltpu.make_async_copy(src, dst, lsem.at[len(local)])
        c.start()
        local[key] = c

    load("br", br_hbm, br_ref)
    load("oc", oc_hbm, oc_ref)
    load("post", post_hbm, post_ref)
    load("x", x_hbm, x_ref)
    load("pre", pre_hbm, pre_ref)
    load("gs", gs_hbm, gs_ref)
    load("us", us_hbm, us_ref)
    for m in range(3):
        load(("w", m), own[m], W.at[m, zl, y])

    def rows_b():
        for key in ("br", "oc", "post"):
            local[key].wait()
        br = br_ref[...].astype(f32)
        inv_b = lax.rsqrt(jnp.mean(br * br, axis=-1, keepdims=True) + eps)
        upst = 0.5 * oc_ref[...].astype(f32) * post_ref[...]
        mean = jnp.mean(upst * br, axis=-1, keepdims=True)
        R[1, tp] = (inv_b * upst - br * (inv_b * inv_b * inv_b) * mean).astype(bf16)

    def rows_n():
        for key in ("x", "pre"):
            local[key].wait()
        xf = x_ref[...].astype(f32)
        inv_x = lax.rsqrt(jnp.mean(xf * xf, axis=-1, keepdims=True) + eps)
        R[0, tp] = (xf * inv_x * pre_ref[...]).astype(bf16)

    ev = [rows_b, rows_n]

    def event(fn, *args):
        ev.append(lambda: fn(*args))

    def enter():
        pl.semaphore_wait(barrier, len(dev))

    event(enter)

    AXES = ("y+", "y-", "z+", "z-")
    NEAR = ((zl, ym), (zl, yp), (zm, y), (zp, y))

    def ag_own(m):
        for to in ("y+", "y-", "z+", "z-"):
            send(("o", m, to), own[m], W.at[m, zl, y], to)

    def ag_forward(m, d):
        to = AXES[d]
        zz, yy = NEAR[d]
        recv(("o", m, to), W.at[m, zz, yy])
        part = W.at[m, zz, yy, ds((GA, GB)[d % 2][m][0])]
        send(("f", m, to) if d in (0, 3) else ("w", m), part, part, to)

    def ag_turn(m, d):
        zz, yy = NEAR[d]
        part = W.at[m, zz, yy, ds((GA, GB)[d // 2][m][0])]
        for to in (("z+", "z-"), ("y+", "y-"))[d // 2]:
            send(("d", m, d % 2, to), part, part, to)

    def ag_mid(m, axis):
        if axis == 0:
            part = W.at[m, zl, y2, ds(GA[m][0])]
            recv(("f", m, "y+"), part)
        else:
            part = W.at[m, z2, y, ds(GB[m][0])]
            recv(("f", m, "z-"), part)
        for to in (("z+", "z-"), ("y+", "y-"))[axis]:
            send(("d", m, 2, to), part, part, to)

    def ag_diag(m, k, d):
        to = AXES[d]
        yk, zk = (ym, yp, y2)[k], (zm, zp, z2)[k]
        zz, yy = ((zk, ym), (zk, yp), (zm, yk), (zp, yk))[d]
        g = (GB, GA)[d // 2][m]
        recv(("d", m, k, to), W.at[m, zz, yy, ds(g[0])])
        part = W.at[m, zz, yy, ds(g[1 + d % 2])]
        send(("w", m), part, part, to)

    def ag_end(m):
        local[("w", m)].wait()
        recv(("w", m), W.at[m, 0])

    for m in range(3):
        event(ag_own, m)
        for d in range(4):
            event(ag_forward, m, d)
            event(ag_turn, m, d)
            for k in range(3):
                event(ag_diag, m, k, d)
        for axis in range(2):
            event(ag_mid, m, axis)
        event(ag_end, m)

    sib = 1 - core
    C = (pl.ds(0, 1024), pl.ds(1024, 1024))
    XS = (("x+", xm), ("x-", xp))

    def rows_own(n):
        r = R.at[n, tp]
        for to in ("x+", "x-", "s"):
            send(("r", n, to) if to != "s" else ("j", n), r, r, to)

    def rows_near(n, d):
        to, xx = XS[d]
        r = R.at[n, xx * 2 + core]
        recv(("r", n, to), r)
        part = R.at[n, xx * 2 + core, :, C[d]]
        send(("rf", n), part, part, to)
        send(("j", n), r, r, "s")

    def rows_far(n):
        r = R.at[n, x2 * 2 + core]
        recv(("rf", n), r)
        send(("j", n), r, r, "s")

    def rows_end(n):
        recv(("j", n), R.at[n, pl.ds(0, 4)])

    for n in range(2):
        event(rows_own, n)
        for d in range(2):
            event(rows_near, n, d)
        event(rows_far, n)
        event(rows_end, n)

    def factors():
        local["gs"].wait()
        local["us"].wait()

        def body(i, _):
            r = pl.ds(pl.multiple_of(i * 32, 32), 32)
            g, u = gs_ref[r, :].astype(f32), us_ref[r, :].astype(f32)
            s = jax.nn.sigmoid(g)
            v = g * s
            silu[r, :] = v
            hid[r, :] = (v * u).astype(bf16)
            dgate[r, :] = u * s * (1.0 + g * (1.0 - s))
            return 0

        lax.fori_loop(0, H // 32, body, 0)

    def partial(m, left, off, n):
        def body(c, _):
            cols = pl.ds(pl.multiple_of(c * 512, 512), 512)
            right = R[n, :, :, cols].reshape(512, 512)
            out = jnp.dot(left[off : off + H, :], right, preferred_element_type=f32).astype(bf16)
            for k in range(4):
                G[m, c, k] = out[:, k * 128 : (k + 1) * 128]
            return 0

        lax.fori_loop(0, 4, body, 0)

    def hidden_grad():
        def body(t, _):
            right = R[1, pl.ds(t * 4, 4)].reshape(256, 2048)
            left = jnp.concatenate([W[0, k // 4, k % 4] for k in range(16)], axis=1)
            hg = lax.dot_general(
                left, right, (((1,), (1,)), ((), ())), preferred_element_type=f32
            )
            cols = pl.ds(pl.multiple_of(t * 256, 256), 256)
            cot[pl.ds(0, H), cols] = (hg * dgate[:, cols]).astype(bf16)
            cot[pl.ds(H, H), cols] = (hg * silu[:, cols]).astype(bf16)
            return 0

        lax.fori_loop(0, 2, body, 0)

    def turn():
        for k in range(11):
            cotT[:, k * 128 : (k + 1) * 128] = cot[k * 128 : (k + 1) * 128, :].T

    def normed_grad(h):
        def body(c, _):
            right = jnp.concatenate(
                [jnp.concatenate([W[1, c, k], W[2, c, k]], axis=0) for k in range(4)], axis=1
            )
            out = jnp.dot(cotT[...], right, preferred_element_type=f32).astype(bf16)
            cols = pl.ds(pl.multiple_of(c * 512, 512), 512)
            NG[:, :, :, cols] = out.reshape(4, 2, 64, 512)
            return 0

        lax.fori_loop(2 * h, 2 * h + 2, body, 0)
        send(("np", h), NG.at[:, sib, :, C[h]], NS.at[:, :, C[h]], "s")

    event(factors)
    event(partial, 0, hid, 0, 1)
    event(hidden_grad)
    event(partial, 1, cot, 0, 0)
    event(partial, 2, cot, H, 0)
    event(turn)
    event(normed_grad, 0)
    event(normed_grad, 1)

    def ng_first(h):
        recv(("np", h), NS.at[:, :, C[h]])
        for k in range(4):
            NG[k, core, :, C[h]] = NG[k, core, :, C[h]] + NS[k, :, C[h]]
        to, back = (("x+", "x-"), ("x-", "x+"))[h]
        send(("n1", h), NG.at[x2, core, :, C[h]], NX1.at[h], to)
        send("n", NG.at[(xm, xp)[h], core, :, C[h]], NXc.at[2 + h], back)

    def ng_second(h):
        to, nxt = (("x+", xp), ("x-", xm))[h]
        recv(("n1", h), NX1.at[h])
        NG[nxt, core, :, C[h]] = NG[nxt, core, :, C[h]] + NX1[h]
        send("n", NG.at[nxt, core, :, C[h]], NXc.at[h], to)

    def ng_end():
        w = []
        recv("n", NXc)
        for h in range(2):
            w.append(
                NG[x, core, :, C[h]].astype(f32) + NXc[h].astype(f32) + NXc[2 + h].astype(f32)
            )
        w = jnp.concatenate(w, axis=1) * pre_ref[...]
        xv = x_ref[...].astype(f32)
        inv = lax.rsqrt(jnp.mean(xv * xv, axis=-1, keepdims=True) + eps)
        ig_ref[...] = (
            oc_ref[...].astype(f32)
            + inv * w
            - xv * (inv * inv * inv) * jnp.mean(w * xv, axis=-1, keepdims=True)
        ).astype(bf16)
        load("ig", ig_ref, ig_hbm)

    for h in range(2):
        event(ng_first, h)
        event(ng_second, h)
    event(ng_end)

    CH = (z2, zp, zm, zl)

    def rs_first_y(m):
        for c in range(4):
            for d, to in ((0, "y+"), (1, "y-")):
                src = G.at[m, CH[c], y2, ds(SP[m][1 + d])]
                send(("a1", m, c, d), src, RY1[m].at[d, c], to)
        for c in range(4):
            for d, to in ((0, "y+"), (1, "y-")):
                src = G.at[m, CH[c], (yp, ym)[d], ds(SP[m][2 - d])]
                send(("C", m, c), src, RYc[m].at[c, 2 + d], to)

    def rs_first_z(m):
        for d, to in ((0, "z+"), (1, "z-")):
            send(("b1", m, d), G.at[m, z2, :, ds(SQ[m][1 + d])], RZ1[m].at[d], to)
        for d, to in ((0, "z+"), (1, "z-")):
            src = G.at[m, (zp, zm)[d], :, ds(SQ[m][2 - d])]
            send(("D", m), src, RZc[m].at[2 + d], to)

    def rs_second_y(m, c, d):
        to, nxt = (("y+", yp), ("y-", ym))[d]
        r = ds(SP[m][1 + d])
        recv(("a1", m, c, d), RY1[m].at[d, c])
        G[m, CH[c], nxt, r] = G[m, CH[c], nxt, r] + RY1[m][d, c]
        send(("C", m, c), G.at[m, CH[c], nxt, r], RYc[m].at[c, d], to)

    def rs_second_z(m, d):
        to, nxt = (("z+", zp), ("z-", zm))[d]
        r = ds(SQ[m][1 + d])
        recv(("b1", m, d), RZ1[m].at[d])
        G[m, nxt, :, r] = G[m, nxt, :, r] + RZ1[m][d]
        send(("D", m), G.at[m, nxt, :, r], RZc[m].at[d], to)

    def add3(a, b, c):
        return (a.astype(f32) + b.astype(f32) + c.astype(f32)).astype(bf16)

    def rs_third_y(m, c):
        recv(("C", m, c), RYc[m].at[c])
        for d in range(2):
            r = ds(SP[m][1 + d])
            G[m, CH[c], y, r] = add3(G[m, CH[c], y, r], RYc[m][c, d], RYc[m][c, 3 - d])
        if c == 0:
            for d, to in ((0, "z+"), (1, "z-")):
                send(("d1", m, d), G.at[m, z2, y, ds(SP[m][1 + d])], SZ1[m].at[d], to)
        elif c < 3:
            d, to = c - 1, ("z+", "z-")[c - 1]
            send(("T", m, 0, 1 - d), G.at[m, CH[c], y, ds(SP[m][2 - d])], SZc[m].at[1 - d, 1], to)

    def rs_third_z(m):
        recv(("D", m), RZc[m])
        for d in range(2):
            r = ds(SQ[m][1 + d])
            if r.size:
                G[m, zl, :, r] = add3(G[m, zl, :, r], RZc[m][d], RZc[m][3 - d])
        for d, to in ((0, "y+"), (1, "y-")):
            send(("c1", m, d), G.at[m, zl, y2, ds(SQ[m][1 + d])], SY1[m].at[d], to)
        for d, to in ((0, "y+"), (1, "y-")):
            src = G.at[m, zl, (yp, ym)[d], ds(SQ[m][2 - d])]
            send(("T", m, 1, 1 - d), src, SYc[m].at[1 - d, 1], to)

    def rs_fourth_y(m, d):
        to, nxt = (("y+", yp), ("y-", ym))[d]
        r = ds(SQ[m][1 + d])
        recv(("c1", m, d), SY1[m].at[d])
        G[m, zl, nxt, r] = G[m, zl, nxt, r] + SY1[m][d]
        send(("T", m, 1, d), G.at[m, zl, nxt, r], SYc[m].at[d, 0], to)

    def rs_fourth_z(m, d):
        to, nxt = (("z+", zp), ("z-", zm))[d]
        r = ds(SP[m][1 + d])
        recv(("d1", m, d), SZ1[m].at[d])
        G[m, nxt, y, r] = G[m, nxt, y, r] + SZ1[m][d]
        send(("T", m, 0, d), G.at[m, nxt, y, r], SZc[m].at[d, 0], to)

    def rs_fifth(m, k, d):
        r = ds((SP, SQ)[k][m][1 + d])
        if not r.size:
            return
        c = (SZc, SYc)[k][m]
        recv(("T", m, k, d), c.at[d])
        T[m, r] = add3(G[m, zl, y, r], c[d, 0], c[d, 1])
        send(("x", m, k, d), T.at[m, r], XF.at[m, r], ("zz+", "zz-")[d])
        load(("out", m, k, d), T.at[m, r], mine[m].at[r])

    def rs_sixth(m, k, d):
        r = ds((SP, SQ)[k][m][1 + d])
        recv(("x", m, k, d), XF.at[m, r])
        send(("z", m), XF.at[m, r], theirs[m].at[r], ("zz+", "zz-")[d])

    def rs_end(m):
        recv(("z", m), theirs[m])

    for m in range(3):
        event(rs_first_y, m)
        event(rs_first_z, m)
        event(rs_third_z, m)
        for c in range(4):
            event(rs_third_y, m, c)
            for d in range(2):
                event(rs_second_y, m, c, d)
        for d in range(2):
            event(rs_second_z, m, d)
            event(rs_fourth_y, m, d)
            event(rs_fourth_z, m, d)
            for k in range(2):
                event(rs_fifth, m, k, d)
                event(rs_sixth, m, k, d)
        event(rs_end, m)

    for k in ORDER:
        ev[k]()
    assert len(ORDER) == len(ev) and len(ids) <= N_RECV
    for c in sends:
        c.wait_send()
    for key in local:
        if key == "ig" or key[0] == "out":
            local[key].wait()


V, SEM = pltpu.VMEM, pltpu.SemaphoreType.DMA
SCRATCH = {
    "W": V((3, 4, 4, H, 128), bf16),
    "R": V((2, 8, 64, 2048), bf16),
    "G": V((3, 4, 4, H, 128), bf16),
    "T": V((3, H, 128), bf16),
    "XF": V((3, H, 128), bf16),
    "silu": V((H, 512), f32),
    "dgate": V((H, 512), f32),
    "hid": V((H, 512), bf16),
    "cot": V((2 * H, 512), bf16),
    "cotT": V((512, 2 * H), bf16),
    "NG": V((4, 2, 64, 2048), bf16),
    "NS": V((4, 64, 2048), bf16),
    "NX1": V((2, 64, 1024), bf16),
    "NXc": V((4, 64, 1024), bf16),
    "x": V((64, 2048), bf16),
    "br": V((64, 2048), bf16),
    "oc": V((64, 2048), bf16),
    "pre": V((1, 2048), f32),
    "post": V((1, 2048), f32),
    "gs": V((H, 512), bf16),
    "us": V((H, 512), bf16),
    "ig": V((64, 2048), bf16),
    "ssem": SEM((N_SEND,)),
    "rsem": SEM((N_RECV,)),
    "lsem": SEM((N_LOCAL,)),
}
for m in range(3):
    p, q = SP[m][1][1], SQ[m][1][1]
    SCRATCH["RY1" + str(m)] = V((2, 4, p, 128), bf16)
    SCRATCH["RYc" + str(m)] = V((4, 4, p, 128), bf16)
    SCRATCH["RZ1" + str(m)] = V((2, 4, max(q, 16), 128), bf16)
    SCRATCH["RZc" + str(m)] = V((4, 4, max(q, 16), 128), bf16)
    SCRATCH["SZ1" + str(m)] = V((2, p, 128), bf16)
    SCRATCH["SZc" + str(m)] = V((2, 2, p, 128), bf16)
    SCRATCH["SY1" + str(m)] = V((2, max(q, 16), 128), bf16)
    SCRATCH["SYc" + str(m)] = V((2, 2, max(q, 16), 128), bf16)


def finish(ig, *refs):
    parts, (ig_out, *outs), (row, both, total, sem) = refs[:6], refs[6:10], refs[10:]
    load = [
        pltpu.make_async_copy(src, both.at[k], sem.at[k]) for k, src in enumerate(parts)
    ]
    load.append(pltpu.make_async_copy(ig, row, sem.at[6]))
    for c in load:
        c.start()
    store = [pltpu.make_async_copy(row, ig_out, sem.at[10])]
    for m in range(3):
        load[m].wait()
        load[3 + m].wait()
        total[m] = both[m].astype(f32) + both[3 + m].astype(f32)
        store.append(pltpu.make_async_copy(total.at[m], outs[m], sem.at[7 + m]))
        store[-1].start()
    load[6].wait()
    store[0].start()
    for c in store:
        c.wait()


def per_device(x, pre, post, gs, us, br, oc, gw, uw, dw):
    hbm = pl.BlockSpec(memory_space=pl.ANY)
    sds = jax.ShapeDtypeStruct
    ig, *pairs = pl.pallas_call(
        kernel,
        out_shape=(sds((64, 2048), bf16), *[sds((H, 128), bf16) for _ in range(6)]),
        in_specs=[hbm] * 10,
        out_specs=(hbm,) * 7,
        scratch_shapes=list(SCRATCH.values()),
        compiler_params=pltpu.CompilerParams(
            collective_id=0, has_side_effects=True, vmem_limit_bytes=67_000_000
        ),
        name="ffn_backward",
    )(x, pre.reshape(1, -1), post.reshape(1, -1), gs.T, us.T, br, oc, gw.T, uw.T, dw.T)
    ig, dg, gg, ug = pl.pallas_call(
        finish,
        out_shape=(sds((64, 2048), bf16), *[sds((H, 128), f32) for _ in range(3)]),
        in_specs=[hbm] * 7,
        out_specs=(hbm,) * 4,
        scratch_shapes=[
            V((64, 2048), bf16), V((6, H, 128), bf16), V((3, H, 128), f32), SEM((11,)),
        ],
        name="finish",
    )(ig, *pairs)
    return ig, gg.T, ug.T, dg.T


def solution(mesh):
    return jax.shard_map(
        per_device,
        mesh=mesh,
        in_specs=(
            P(("rep", "fs", "tp"), None),
            P(),
            P(),
            P(("rep", "fs"), "tp"),
            P(("rep", "fs"), "tp"),
            P(("rep", "fs", "tp"), None),
            P(("rep", "fs", "tp"), None),
            P("fs", "tp"),
            P("fs", "tp"),
            P("fs", "tp"),
        ),
        out_specs=(P(("rep", "fs", "tp"), None), P("fs", "tp"), P("fs", "tp"), P("fs", "tp")),
        check_vma=False,
    )
```

time: 371 us -> 122 us (0.33)
  waiting for transfers between devices: 264 us -> 0 us
  Pallas kernels: 0 us -> 121 us
  local copies, waits for them, and re-layouts: 34.6 us -> 0 us
  matrix products: 22.9 us -> 0 us
  starting transfers between devices: 17.9 us -> 0 us
  other arithmetic: 14.4 us -> 0 us
  between operations: 14 us -> 0.64 us
    all_gather x2 -> x0, waiting for transfers between devices: 143 us -> none  [the longest x1 108 us: side_by_side(): whole = lax.all_gather(both, axis, axis=dim, tiled=True)]
    pallas_call x0 -> x2, Pallas kernels: none -> 121 us  [the longest x1 119 us: per_device(): pl.pallas_call(kernel, out_shape=(sds((64, 2048), bf16), *[sds((H, 128),...]
    unnamed x4 -> x0, waiting for transfers between devices: 96.7 us -> none
    all_to_all x4 -> x0, waiting for transfers between devices: 24.4 us -> none  [the longest x3 24.4 us: copy_for_each(): lax.all_to_all(jnp.broadcast_to(shard[None], (size, *shard.shape)), axis,...]
    dot_general x6 -> x0, matrix products: 22.9 us -> none  [the longest x2 9.08 us: contract_cols(): lax.dot_general(left, right, (((1,), (1,)), ((), ())), preferred_element_...]
    all_to_all x4 -> x0, starting transfers between devices: 17.8 us -> none  [the longest x3 13 us: copy_for_each(): lax.all_to_all(jnp.broadcast_to(shard[None], (size, *shard.shape)), axis,...]
    unnamed x34 -> x0, local copies, waits for them, and re-layouts: 14.4 us -> none
    another operation x2 -> x0, local copies, waits for them, and re-layouts: 6.2 us -> none  [joined_along(): return jnp.moveaxis(blocks, 0, dim).reshape(lengths)]
  transfers between devices with their start and end apart: 7 -> 0, of which waited for: 6 -> 0; matrix products, arithmetic and copies ran while one was open for 10% -> 0% of each run, Pallas kernels for 0% -> 0%
where the time goes in v2:
time: 122 us
  Pallas kernels  121 us (99%)
    pallas_call x1, Pallas kernels, per_device(): pl.pallas_call(kernel, out_shape=(sds((64, 2048), bf16), *[sds((H, 128),...  119 us

profile of v2, /device:TPU:6, one launch (start us, length us, event | category | flops | bytes accessed | tf_op | source)
XLA Modules:
  0.0 121.8 jit_solution(16704808848846141644)
XLA Ops:
  0.6 118.8 %ffn_backward.1 = (bf16[64,2048]{1,0:T(8,128)(2,1)}, bf16[704,128]{1,0:T(8,128)(2,1)}, bf16[704,128]{1,0:T(8,128)(2,1)}, bf16[704,128]{1,0:T(8,128)(2,1)}, bf16[...) custom-call(bf16[64,2048]{1,0:T(8,128)(2,1)} %x_hbm.1, f32[1,2048]{1,0:T(1,128)} %bitcast.15, ...), custom_call_target="tpu_custom_call" | custom-call | tf_op jit(solution)/shard_map/ffn_backward/pallas_call | solution.py:534
  119.4 2.4 %finish.1 = (bf16[64,2048]{1,0:T(8,128)(2,1)}, f32[704,128]{1,0:T(8,128)}, f32[704,128]{1,0:T(8,128)}, f32[704,128]{1,0:T(8,128)}) custom-call(bf16[64,2048]{1,0:T(8,128)(2,1)} %get-tuple-element.15.ig, bf16[704,128]{1,0:T(8,128)(2,1)} %get-tuple-element.16.refs_0_, bf16[704,128]{1,0:T(8,128)(2,1)} %get-tuple-element.17.refs_1_, ...), custom_call_target="tpu_custom_call" | custom-call | tf_op jit(solution)/shard_map/finish/pallas_call | solution.py:545

commit v3 on v2

v3 whole, which is shorter than its diff:
```python
import jax
import jax.numpy as jnp
from jax import lax
from jax.experimental import pallas as pl
from jax.experimental.pallas import tpu as pltpu
from jax.sharding import PartitionSpec as P

MESH = pl.DeviceIdType.MESH
bf16, f32 = jnp.bfloat16, jnp.float32
eps = 1e-06

HU = 352
QU = HU // 2
NQ = (192, 192, 128)
N_RECV, N_SEND, N_LOCAL = 108, 48, 20
ORDER = (
    2, 12, 0, 38, 1, 30, 47, 21, 13, 16, 14, 22, 3, 25, 40, 17, 15, 46, 39, 4, 26, 32, 18, 7, 31,
    41, 23, 42, 19, 5, 8, 24, 43, 6, 33, 27, 34, 9, 35, 28, 44, 10, 48, 45, 49, 62, 76, 11, 36, 50,
    37, 52, 122, 65, 77, 108, 63, 51, 69, 67, 85, 99, 29, 53, 123, 66, 20, 55, 64, 78, 70, 100, 68,
    111, 124, 58, 71, 113, 54, 115, 112, 109, 101, 56, 114, 125, 72, 116, 86, 110, 59, 88, 102, 90,
    92, 126, 87, 73, 117, 89, 91, 93, 79, 57, 103, 127, 94, 74, 118, 128, 104, 80, 95, 105, 75, 81,
    119, 60, 129, 96, 82, 120, 97, 106, 83, 61, 121, 98, 84, 130, 107,
)


def mod(a, n):
    return lax.rem(a + n, n)


def kernel(
    x_hbm, pre_hbm, post_hbm, gs_hbm, us_hbm, br_hbm, oc_hbm, gw_hbm, uw_hbm, dw_hbm,
    ig_hbm, d_out, g_out, u_out,
    *scratch,
):
    s = dict(zip(SCRATCH, scratch))
    W, R, G, GU, silu, dgate, hid = (s[k] for k in ("W", "R", "G", "GU", "si", "dg", "hid"))
    cot, cotT, NG, NS, NX1, NXc = (s[k] for k in ("cot", "cotT", "NG", "NS", "NX1", "NXc"))
    NB, NC = s["NB"], s["NC"]
    RY1, RYo, S, M4, MR, T, XF, K4, KR, KS, U1, UR, TQ, XQ = (
        [s[k, m] for m in range(3)] for k in BUFS
    )
    x_ref, pre_ref, post_ref, br_ref, oc_ref, ig_ref = (
        s[k] for k in ("x", "pre", "post", "br", "oc", "ig")
    )
    ssem, rsem, lsem = s["ssem"], s["rsem"], s["lsem"]
    out = (d_out, g_out, u_out)
    rep, fs, tp = lax.axis_index("rep"), lax.axis_index("fs"), lax.axis_index("tp")
    zl, y = fs // 4, fs % 4
    z = rep * 4 + zl
    x, core = tp // 2, tp % 2
    sib = 1 - core
    half = y // 2
    mate, cross = y + 1 - 2 * (y % 2), 3 - y
    diag = 3 - mate
    zm, zp, z2 = mod(zl - 1, 4), mod(zl + 1, 4), mod(zl + 2, 4)
    xm, xp, x2 = mod(x - 1, 4), mod(x + 1, 4), mod(x + 2, 4)

    def zdev(d):
        zz = mod(z + d, 8)
        return {"rep": zz // 4, "fs": (zz % 4) * 4 + y}

    dev = {
        "m": {"fs": zl * 4 + mate},
        "c": {"fs": zl * 4 + cross},
        "z+": zdev(1),
        "z-": zdev(-1),
        "zz+": zdev(2),
        "zz-": zdev(-2),
        "x+": {"tp": xp * 2 + core},
        "x-": {"tp": xm * 2 + core},
        "s": {"tp": x * 2 + sib},
    }
    ZS = ("z+", "z-")
    XS = ("x+", "x-")

    barrier = pltpu.get_barrier_semaphore()
    for name in dev:
        pl.semaphore_signal(barrier, inc=1, device_id=dev[name], device_id_type=MESH)

    ids = {}
    sends = []
    count = [0]

    def number(key):
        return ids.setdefault(key, len(ids))

    def send(key, src, dst, to):
        if len(sends) == N_SEND:
            sends.pop(0).wait_send()
        c = pltpu.make_async_remote_copy(
            src_ref=src, dst_ref=dst, send_sem=ssem.at[count[0] % N_SEND],
            recv_sem=rsem.at[number(key)], device_id=dev[to], device_id_type=MESH,
        )
        c.start()
        count[0] += 1
        sends.append(c)

    def recv(key, ref):
        pltpu.make_async_copy(ref, ref, rsem.at[number(key)]).wait()

    own = (dw_hbm, gw_hbm, uw_hbm)
    local = {}

    def load(key, src, dst):
        c = pltpu.make_async_copy(src, dst, lsem.at[len(local)])
        c.start()
        local[key] = c

    mine = pl.ds(pl.multiple_of(half * HU, 32), HU)
    other = pl.ds(pl.multiple_of((1 - half) * HU, 32), HU)
    load("br", br_hbm, br_ref)
    load("oc", oc_hbm, oc_ref)
    load("post", post_hbm, post_ref)
    load("x", x_hbm, x_ref)
    load("pre", pre_hbm, pre_ref)
    load("gs", gs_hbm.at[mine], GU.at[0, 0])
    load("us", us_hbm.at[mine], GU.at[0, 1])
    for m in range(3):
        load(("w", m), own[m].at[mine], W.at[m, zl, y])

    def rows_b():
        for key in ("br", "oc", "post"):
            local[key].wait()
        br = br_ref[...].astype(f32)
        inv_b = lax.rsqrt(jnp.mean(br * br, axis=-1, keepdims=True) + eps)
        upst = 0.5 * oc_ref[...].astype(f32) * post_ref[...]
        mean = jnp.mean(upst * br, axis=-1, keepdims=True)
        R[1, 0, tp] = (inv_b * upst - br * (inv_b * inv_b * inv_b) * mean).astype(bf16)

    def rows_n():
        for key in ("x", "pre"):
            local[key].wait()
        xf = x_ref[...].astype(f32)
        inv_x = lax.rsqrt(jnp.mean(xf * xf, axis=-1, keepdims=True) + eps)
        R[0, 0, tp] = (xf * inv_x * pre_ref[...]).astype(bf16)

    ev = [rows_b, rows_n]

    def event(fn, *args):
        ev.append(lambda: fn(*args))

    def enter():
        pl.semaphore_wait(barrier, len(dev))

    event(enter)

    def ag_own(m):
        w = own[m].at[mine]
        send(("o", m), w, W.at[m, zl, y], "m")
        send(("c", m), own[m].at[other], W.at[m, zl, y], "c")
        for to in ZS:
            send(("z", m, 0), w, W.at[m, zl, y], to)

    def ag_y(m, k):
        yy = (mate, cross, diag)[k]
        w = W.at[m, zl, yy]
        recv((("o", m), ("c", m), ("d", m))[k], w)
        if k == 1:
            send(("d", m), w, w, "m")
        for to in ZS:
            send(("z", m, k + 1), w, w, to)

    Q = (pl.ds(0, QU), pl.ds(QU, QU))

    def ag_z(m, k):
        yy = (y, mate, cross, diag)[k]
        recv(("z", m, k), W.at[m, 0, pl.ds(0, 2)])
        for d in range(2):
            w = W.at[m, (zm, zp)[d], yy, Q[d]]
            send(("w", m), w, w, ZS[d])

    def ag_end(m):
        local[("w", m)].wait()
        recv(("w", m), W.at[m, z2])

    for m in range(3):
        event(ag_own, m)
        for k in range(3):
            event(ag_y, m, k)
        for k in range(4):
            event(ag_z, m, k)
        event(ag_end, m)

    C = (pl.ds(0, 1024), pl.ds(1024, 1024))

    def rows_own(n):
        r = R.at[n, 0, tp]
        send(("rc", n), r, R.at[n, 1, tp], "c")
        rows_out(n, 0)

    def rows_cross(n):
        recv(("rc", n), R.at[n, 1, tp])
        rows_out(n, 1)

    def rows_out(n, b):
        r = R.at[n, b, tp]
        for to in XS:
            send(("r", n, b), r, r, to)
        send(("j", n, b), r, r, "s")

    def rows_near(n, b):
        recv(("r", n, b), R.at[n, b, pl.ds(0, 2)])
        for d in range(2):
            slot = (xm, xp)[d] * 2 + core
            r = R.at[n, b, slot, :, C[d]]
            send(("rf", n, b), r, r, XS[d])
        for d in range(2):
            r = R.at[n, b, (xm, xp)[d] * 2 + core]
            send(("j", n, b), r, r, "s")

    def rows_far(n, b):
        r = R.at[n, b, x2 * 2 + core]
        recv(("rf", n, b), r)
        send(("j", n, b), r, r, "s")

    def rows_end(n, b):
        recv(("j", n, b), R.at[n, b, pl.ds(0, 4)])

    for n in range(2):
        event(rows_own, n)
        event(rows_cross, n)
        for b in range(2):
            event(rows_near, n, b)
            event(rows_far, n, b)
            event(rows_end, n, b)

    def gates_out():
        send("gu", gs_hbm.at[other], GU.at[1, 0], "c")
        send("gu", us_hbm.at[other], GU.at[1, 1], "c")

    def factors(b):
        if b == 0:
            local["gs"].wait()
            local["us"].wait()
        else:
            recv("gu", GU.at[1])
        cols = pl.ds(b * 512, 512)

        def body(i, _):
            r = pl.ds(pl.multiple_of(i * 32, 32), 32)
            g, u = GU[b, 0, r, :].astype(f32), GU[b, 1, r, :].astype(f32)
            sg = jax.nn.sigmoid(g)
            v = g * sg
            silu[r, cols] = v
            hid[r, cols] = (v * u).astype(bf16)
            dgate[r, cols] = u * sg * (1.0 + g * (1.0 - sg))
            return 0

        lax.fori_loop(0, HU // 32, body, 0)

    def partial(m, left, off, n):
        def body(c, _):
            cols = pl.ds(pl.multiple_of(c * 512, 512), 512)
            right = R[n, :, :, :, cols].reshape(1024, 512)
            g = jnp.dot(left[off : off + HU, :], right, preferred_element_type=f32).astype(bf16)
            for k in range(4):
                G[m, c, k] = g[:, k * 128 : (k + 1) * 128]
            return 0

        lax.fori_loop(0, 4, body, 0)

    def hidden_grad():
        def body(t, _):
            right = R[1, t // 2, pl.ds((t % 2) * 4, 4)].reshape(256, 2048)
            left = jnp.concatenate([W[0, k // 4, k % 4] for k in range(16)], axis=1)
            hg = lax.dot_general(
                left, right, (((1,), (1,)), ((), ())), preferred_element_type=f32
            )
            cols = pl.ds(pl.multiple_of(t * 256, 256), 256)
            cot[pl.ds(0, HU), cols] = (hg * dgate[:, cols]).astype(bf16)
            cot[pl.ds(HU, HU), cols] = (hg * silu[:, cols]).astype(bf16)
            return 0

        lax.fori_loop(0, 4, body, 0)

    def turn():
        for k in range(8):
            cotT[k * 128 : (k + 1) * 128, :] = cot[:, k * 128 : (k + 1) * 128].T

    def normed_grad(h):
        def body(c, _):
            right = jnp.concatenate(
                [jnp.concatenate([W[1, c, k], W[2, c, k]], axis=0) for k in range(4)], axis=1
            )
            g = jnp.dot(cotT[...], right, preferred_element_type=f32).astype(bf16)
            cols = pl.ds(pl.multiple_of(c * 512, 512), 512)
            NG[:, :, :, :, cols] = g.reshape(2, 4, 2, 64, 512)
            return 0

        lax.fori_loop(2 * h, 2 * h + 2, body, 0)
        send(("np", h), NG.at[:, :, sib, :, C[h]], NS.at[:, :, :, C[h]], "s")

    event(gates_out)
    event(factors, 0)
    event(factors, 1)
    event(partial, 0, hid, 0, 1)
    event(hidden_grad)
    event(partial, 1, cot, 0, 0)
    event(partial, 2, cot, HU, 0)
    event(turn)
    event(normed_grad, 0)
    event(normed_grad, 1)

    def ng_first(h):
        recv(("np", h), NS.at[:, :, :, C[h]])
        for b in range(2):
            for k in range(4):
                NG[b, k, core, :, C[h]] = NG[b, k, core, :, C[h]] + NS[b, k, :, C[h]]
        send(("n1", h), NG.at[:, x2, core, :, C[h]], NX1.at[h], XS[h])
        send("n", NG.at[:, (xm, xp)[h], core, :, C[h]], NXc.at[2 + h], XS[1 - h])

    def ng_second(h):
        nxt = (xp, xm)[h]
        recv(("n1", h), NX1.at[h])
        for b in range(2):
            NG[b, nxt, core, :, C[h]] = NG[b, nxt, core, :, C[h]] + NX1[h, b]
        send("n", NG.at[:, nxt, core, :, C[h]], NXc.at[h], XS[h])

    def ng_sum(b):
        return jnp.concatenate(
            [
                NG[b, x, core, :, C[h]].astype(f32)
                + NXc[h, b].astype(f32)
                + NXc[2 + h, b].astype(f32)
                for h in range(2)
            ],
            axis=1,
        )

    def ng_third():
        recv("n", NXc)
        NB[...] = ng_sum(1).astype(bf16)
        send("nc", NB, NC, "c")

    def ng_end():
        recv("nc", NC)
        w = (ng_sum(0) + NC[...].astype(f32)) * pre_ref[...]
        xv = x_ref[...].astype(f32)
        inv = lax.rsqrt(jnp.mean(xv * xv, axis=-1, keepdims=True) + eps)
        ig_ref[...] = (
            oc_ref[...].astype(f32)
            + inv * w
            - xv * (inv * inv * inv) * jnp.mean(w * xv, axis=-1, keepdims=True)
        ).astype(bf16)
        load("ig", ig_ref, ig_hbm)

    for h in range(2):
        event(ng_first, h)
        event(ng_second, h)
    event(ng_third)
    event(ng_end)

    CH = (zl, zm, zp, z2)
    OWN = {k: (mod(zl + k, 4), mod(z + k, 8) // 4) for k in (4, 3, 2, 1, -1, -2, -3)}

    def add3(a, b, c):
        return (a.astype(f32) + b.astype(f32) + c.astype(f32)).astype(bf16)

    def from_rep(d):
        return mod(z + (-2, 2)[d], 8) // 4

    def rs_first(m):
        p = pl.ds(0, HU - NQ[m])
        for c in range(4):
            send(("a", m, c), G.at[m, CH[c], diag, p], RY1[m].at[c], "m")
        for c in range(4):
            send(("C", m, c), G.at[m, CH[c], mate, p], RYo[m].at[c], "m")

    def rs_second(m, c):
        p = pl.ds(0, HU - NQ[m])
        recv(("a", m, c), RY1[m].at[c])
        G[m, CH[c], cross, p] = G[m, CH[c], cross, p] + RY1[m][c]
        send(("C", m, c), G.at[m, CH[c], cross, p], S[m].at[CH[c], half], "c")

    def rs_third(m, c):
        p = pl.ds(0, HU - NQ[m])
        recv(("C", m, c), S[m].at[CH[c]])
        S[m][CH[c], half] = G[m, CH[c], y, p] + RYo[m][c]
        if c == 0:
            slot, h = OWN[4]
            for d in range(2):
                send(("M", m, 4), S[m].at[slot, h, part(m, d)], M4[m].at[d], ZS[d])

    def part(m, d):
        n = (HU - NQ[m]) // 2
        return pl.ds(d * n, n)

    def rs_ring(m, k):
        recv(("M", m, k + 1), M4[m] if k == 3 else MR[m].at[2 - k])
        for d in range(2):
            slot, h = OWN[(k, -k)[d]]
            if k == 3:
                r = part(m, d)
                S[m][slot, h, r] = S[m][slot, h, r] + M4[m][d]
            else:
                S[m][slot, h] = S[m][slot, h] + MR[m][2 - k, d]
            send(("M", m, k), S[m].at[slot, h], MR[m].at[3 - k, d], ZS[d])

    def rows_at(start, n):
        return pl.ds(pl.multiple_of(start, 16), n)

    def rs_own(m):
        recv(("M", m, 1), MR[m].at[2])
        T[m][...] = add3(S[m][zl, rep], MR[m][2, 0], MR[m][2, 1])
        for d in range(2):
            r = part(m, d)
            send(("x", m), T[m].at[r], XF[m].at[r], ("zz+", "zz-")[d])
        load(("out", m), T[m], out[m].at[rows_at(rep * HU, HU - NQ[m])])

    def rs_swap(m):
        recv(("x", m), XF[m])
        n = (HU - NQ[m]) // 2
        for d in range(2):
            dst = out[m].at[rows_at(from_rep(d) * HU + d * n, n)]
            send(("e", m), XF[m].at[part(m, d)], dst, ("zz+", "zz-")[d])

    def rows_q(m, h, d, parts):
        n = NQ[m]
        return rows_at(HU - n + h * (n // 2) + d * (n // 4), n // parts)

    def qs_first(m):
        slot, h = OWN[4]
        for d in range(2):
            send(("K", m, 4), G.at[m, slot, :, rows_q(m, h, d, 4)], K4[m].at[d], ZS[d])

    def qs_ring(m, k):
        recv(("K", m, k + 1), K4[m] if k == 3 else KR[m].at[2 - k])
        for d in range(2):
            slot, h = OWN[(k, -k)[d]]
            if k == 3:
                r = rows_q(m, h, d, 4)
                G[m, slot, :, r] = G[m, slot, :, r] + K4[m][d]
            else:
                r = rows_q(m, h, 0, 2)
                G[m, slot, :, r] = G[m, slot, :, r] + KR[m][2 - k, d]
            src = G.at[m, slot, :, rows_q(m, h, 0, 2)]
            send(("K", m, k), src, KR[m].at[3 - k, d], ZS[d])

    def qs_own(m):
        recv(("K", m, 1), KR[m].at[2])
        KS[m][...] = add3(G[m, zl, :, rows_q(m, rep, 0, 2)], KR[m][2, 0], KR[m][2, 1])
        send(("u", m), KS[m].at[diag], U1[m], "m")
        send(("U", m), KS[m].at[mate], UR[m].at[0], "m")

    def qs_cross(m):
        recv(("u", m), U1[m])
        KS[m][cross] = KS[m][cross] + U1[m][...]
        send(("U", m), KS[m].at[cross], UR[m].at[1], "c")

    def qs_sum(m):
        recv(("U", m), UR[m])
        TQ[m][half] = KS[m][y] + UR[m][0]
        TQ[m][1 - half] = UR[m][1]
        n = NQ[m] // 2
        for d in range(2):
            send(("v", m), TQ[m].at[d], XQ[m].at[d], ("zz+", "zz-")[d])
            load(("out", m, d), TQ[m].at[d], out[m].at[rows_at((d + 1) * HU - 2 * n + rep * n, n)])

    def qs_swap(m):
        recv(("v", m), XQ[m])
        n = NQ[m] // 2
        for d in range(2):
            dst = out[m].at[rows_at((d + 1) * HU - 2 * n + from_rep(d) * n, n)]
            send(("e", m), XQ[m].at[d], dst, ("zz+", "zz-")[d])

    def rs_end(m):
        recv(("e", m), G.at[m, 0, 0])

    for m in range(3):
        event(rs_first, m)
        for c in range(4):
            event(rs_second, m, c)
            event(rs_third, m, c)
        for k in (3, 2, 1):
            event(rs_ring, m, k)
        event(rs_own, m)
        event(rs_swap, m)
        event(qs_first, m)
        for k in (3, 2, 1):
            event(qs_ring, m, k)
        event(qs_own, m)
        event(qs_cross, m)
        event(qs_sum, m)
        event(qs_swap, m)
        event(rs_end, m)

    for k in ORDER:
        ev[k]()
    assert sorted(ORDER) == list(range(len(ev))) and len(ids) <= N_RECV
    for c in sends:
        c.wait_send()
    for key in local:
        if key == "ig" or key[0] == "out":
            local[key].wait()


V, SEM = pltpu.VMEM, pltpu.SemaphoreType.DMA
SCRATCH = {
    "W": V((3, 4, 4, HU, 128), bf16),
    "R": V((2, 2, 8, 64, 2048), bf16),
    "G": V((3, 4, 4, HU, 128), bf16),
    "GU": V((2, 2, HU, 512), bf16),
    "si": V((HU, 1024), f32),
    "dg": V((HU, 1024), f32),
    "hid": V((HU, 1024), bf16),
    "cot": V((2 * HU, 1024), bf16),
    "cotT": V((1024, 2 * HU), bf16),
    "NG": V((2, 4, 2, 64, 2048), bf16),
    "NS": V((2, 4, 64, 2048), bf16),
    "NX1": V((2, 2, 64, 1024), bf16),
    "NXc": V((4, 2, 64, 1024), bf16),
    "NB": V((64, 2048), bf16),
    "NC": V((64, 2048), bf16),
    "x": V((64, 2048), bf16),
    "br": V((64, 2048), bf16),
    "oc": V((64, 2048), bf16),
    "ig": V((64, 2048), bf16),
    "pre": V((1, 2048), f32),
    "post": V((1, 2048), f32),
    "ssem": SEM((N_SEND,)),
    "rsem": SEM((N_RECV,)),
    "lsem": SEM((N_LOCAL,)),
}


BUFS = ("RY1", "RYo", "S", "M4", "MR", "T", "XF", "K4", "KR", "KS", "U1", "UR", "TQ", "XQ")
for m in range(3):
    p, h = HU - NQ[m], NQ[m] // 2
    shapes = (
        (4, p), (4, p), (4, 2, p), (2, p // 2), (3, 2, p), (p,), (p,),
        (2, 4, h // 2), (3, 2, 4, h), (4, h), (h,), (2, h), (2, h), (2, h),
    )
    for k, shape in zip(BUFS, shapes):
        SCRATCH[k, m] = V((*shape, 128), bf16)


def finish(*refs):
    ins, outs, (row, half, full, sem) = refs[:4], refs[4:8], refs[8:]
    bufs = [row] + [half.at[m] for m in range(3)]
    res = [row] + [full.at[m] for m in range(3)]
    loads = [pltpu.make_async_copy(ins[k], bufs[k], sem.at[k]) for k in range(4)]
    stores = [pltpu.make_async_copy(res[k], outs[k], sem.at[4 + k]) for k in range(4)]
    for c in loads:
        c.start()
    for k in range(4):
        loads[k].wait()
        if k:
            full[k - 1] = half[k - 1].astype(f32)
        stores[k].start()
    for c in stores:
        c.wait()


def per_device(x, pre, post, gs, us, br, oc, gw, uw, dw):
    hbm = pl.BlockSpec(memory_space=pl.ANY)
    sds = jax.ShapeDtypeStruct
    parts = pl.pallas_call(
        kernel,
        out_shape=(sds((64, 2048), bf16), *[sds((2 * HU, 128), bf16)] * 3),
        in_specs=[hbm] * 10,
        out_specs=(hbm,) * 4,
        scratch_shapes=list(SCRATCH.values()),
        compiler_params=pltpu.CompilerParams(
            collective_id=0, has_side_effects=True, vmem_limit_bytes=67_000_000
        ),
        name="ffn_backward",
    )(x, pre.reshape(1, -1), post.reshape(1, -1), gs.T, us.T, br, oc, gw.T, uw.T, dw.T)
    ig, dg, gg, ug = pl.pallas_call(
        finish,
        out_shape=(sds((64, 2048), bf16), *[sds((2 * HU, 128), f32)] * 3),
        in_specs=[hbm] * 4,
        out_specs=(hbm,) * 4,
        scratch_shapes=[
            V((64, 2048), bf16), V((3, 2 * HU, 128), bf16), V((3, 2 * HU, 128), f32), SEM((8,)),
        ],
        name="finish",
    )(*parts)
    return ig, gg.T, ug.T, dg.T


def solution(mesh):
    return jax.shard_map(
        per_device,
        mesh=mesh,
        in_specs=(
            P(("rep", "fs", "tp"), None),
            P(),
            P(),
            P(("rep", "fs"), "tp"),
            P(("rep", "fs"), "tp"),
            P(("rep", "fs", "tp"), None),
            P(("rep", "fs", "tp"), None),
            P("fs", "tp"),
            P("fs", "tp"),
            P("fs", "tp"),
        ),
        out_specs=(P(("rep", "fs", "tp"), None), P("fs", "tp"), P("fs", "tp"), P("fs", "tp")),
        check_vma=False,
    )
```

time: 122 us -> 102 us (0.84); the launches traced: 122 us -> 100 us
  Pallas kernels: 121 us -> 99.7 us
    pallas_call x2, Pallas kernels: 121 us -> 99.7 us  [the longest x1 97.7 us: per_device(): pl.pallas_call(kernel, out_shape=(sds((64, 2048), bf16), *[sds((2 * HU, 1...]
where the time goes in v3:
time: 102 us; the launch traced here: 100 us
  Pallas kernels  99.7 us (98%)
    pallas_call x1, Pallas kernels, per_device(): pl.pallas_call(kernel, out_shape=(sds((64, 2048), bf16), *[sds((2 * HU, 1...  97.7 us
    pallas_call x1, Pallas kernels, per_device(): pl.pallas_call(finish, out_shape=(sds((64, 2048), bf16), *[sds((2 * HU, 1...  2.08 us

profile of v3, /device:TPU:6, one launch (start us, length us, event | category | flops | bytes accessed | tf_op | source)
XLA Modules:
  0.0 100.4 jit_solution(18240786198368150271)
XLA Ops:
  0.6 97.7 %ffn_backward.1 = (bf16[64,2048]{1,0:T(8,128)(2,1)}, bf16[704,128]{1,0:T(8,128)(2,1)}, bf16[704,128]{1,0:T(8,128)(2,1)}, bf16[704,128]{1,0:T(8,128)(2,1)}) custom-call(bf16[64,2048]{1,0:T(8,128)(2,1)} %x_hbm.1, f32[1,2048]{1,0:T(1,128)} %bitcast.15, f32[1,2048]{1,0:T(1,128)} %bitcast.16, bf16[704,512]{1,0:T(8,128)(2,1)} %bitcast.10, ...), custom_call_target="tpu_custom_call" | custom-call | tf_op jit(solution)/shard_map/ffn_backward/pallas_call | solution.py:557
  98.3 2.1 %finish.1 = (bf16[64,2048]{1,0:T(8,128)(2,1)}, f32[704,128]{1,0:T(8,128)}, f32[704,128]{1,0:T(8,128)}, f32[704,128]{1,0:T(8,128)}) custom-call(bf16[64,2048]{1,0:T(8,128)(2,1)} %get-tuple-element.12.refs_0_, bf16[704,128]{1,0:T(8,128)(2,1)} %get-tuple-element.13.refs_1_, bf16[704,128]{1,0:T(8,128)(2,1)} %get-tuple-element.14.refs_2_, ...), custom_call_target="tpu_custom_call" | custom-call | tf_op jit(solution)/shard_map/finish/pallas_call | solution.py:568

commit v4 on v3

--- a/solution.py
+++ b/solution.py
@@ -11,15 +11,16 @@
 
 HU = 352
 QU = HU // 2
-NQ = (192, 192, 128)
+NQ = (192, 192, 192)
 N_RECV, N_SEND, N_LOCAL = 108, 48, 20
 ORDER = (
-    2, 12, 0, 38, 1, 30, 47, 21, 13, 16, 14, 22, 3, 25, 40, 17, 15, 46, 39, 4, 26, 32, 18, 7, 31,
-    41, 23, 42, 19, 5, 8, 24, 43, 6, 33, 27, 34, 9, 35, 28, 44, 10, 48, 45, 49, 62, 76, 11, 36, 50,
-    37, 52, 122, 65, 77, 108, 63, 51, 69, 67, 85, 99, 29, 53, 123, 66, 20, 55, 64, 78, 70, 100, 68,
-    111, 124, 58, 71, 113, 54, 115, 112, 109, 101, 56, 114, 125, 72, 116, 86, 110, 59, 88, 102, 90,
-    92, 126, 87, 73, 117, 89, 91, 93, 79, 57, 103, 127, 94, 74, 118, 128, 104, 80, 95, 105, 75, 81,
-    119, 60, 129, 96, 82, 120, 97, 106, 83, 61, 121, 98, 84, 130, 107,
+    2, 3, 21, 0, 38, 47, 12, 1, 30, 4, 5, 22, 23, 25, 16, 40, 8, 6, 39, 24, 9, 14, 32, 26, 46, 27,
+    41, 7, 13, 15, 42, 31, 10, 43, 28, 33, 18, 34, 17, 35, 19, 11, 44, 29, 48, 45, 49, 36, 50, 85,
+    51, 52, 37, 54, 108, 58, 131, 59, 60, 86, 61, 72, 53, 74, 117, 20, 55, 56, 109, 57, 94, 132, 95,
+    76, 71, 118, 120, 87, 122, 62, 64, 110, 124, 78, 119, 133, 123, 67, 125, 63, 88, 101, 97, 99,
+    96, 134, 65, 102, 98, 73, 121, 126, 89, 100, 103, 68, 77, 111, 75, 79, 135, 90, 80, 127, 104,
+    136, 91, 66, 112, 81, 137, 128, 105, 113, 92, 82, 114, 138, 129, 69, 106, 83, 115, 130, 107, 84,
+    70, 139, 116, 93,
 )
 
 
@@ -248,30 +249,30 @@
 
         lax.fori_loop(0, HU // 32, body, 0)
 
-    def partial(m, left, off, n):
-        def body(c, _):
-            cols = pl.ds(pl.multiple_of(c * 512, 512), 512)
-            right = R[n, :, :, :, cols].reshape(1024, 512)
-            g = jnp.dot(left[off : off + HU, :], right, preferred_element_type=f32).astype(bf16)
-            for k in range(4):
-                G[m, c, k] = g[:, k * 128 : (k + 1) * 128]
-            return 0
-
-        lax.fori_loop(0, 4, body, 0)
+    CH = (zl, zm, zp, z2)
+
+    def partial(m, c):
+        n, left = ((1, hid), (0, cot.at[:HU]), (0, cot.at[HU:]))[m]
+        cols = pl.ds(pl.multiple_of(CH[c] * 512, 512), 512)
+        right = R[n, :, :, :, cols].reshape(1024, 512)
+        g = jnp.dot(left[...], right, preferred_element_type=f32).astype(bf16)
+        for k in range(4):
+            G[m, CH[c], k] = g[:, k * 128 : (k + 1) * 128]
+        send(("a", m, c), G.at[m, CH[c], diag, pl.ds(0, HU - NQ[m])], RY1[m].at[c], "m")
 
     def hidden_grad():
         def body(t, _):
-            right = R[1, t // 2, pl.ds((t % 2) * 4, 4)].reshape(256, 2048)
+            right = R[1, t].reshape(512, 2048)
             left = jnp.concatenate([W[0, k // 4, k % 4] for k in range(16)], axis=1)
             hg = lax.dot_general(
                 left, right, (((1,), (1,)), ((), ())), preferred_element_type=f32
             )
-            cols = pl.ds(pl.multiple_of(t * 256, 256), 256)
+            cols = pl.ds(pl.multiple_of(t * 512, 512), 512)
             cot[pl.ds(0, HU), cols] = (hg * dgate[:, cols]).astype(bf16)
             cot[pl.ds(HU, HU), cols] = (hg * silu[:, cols]).astype(bf16)
             return 0
 
-        lax.fori_loop(0, 4, body, 0)
+        lax.fori_loop(0, 2, body, 0)
 
     def turn():
         for k in range(8):
@@ -293,10 +294,10 @@
     event(gates_out)
     event(factors, 0)
     event(factors, 1)
-    event(partial, 0, hid, 0, 1)
     event(hidden_grad)
-    event(partial, 1, cot, 0, 0)
-    event(partial, 2, cot, HU, 0)
+    for m in range(3):
+        for c in range(4):
+            event(partial, m, c)
     event(turn)
     event(normed_grad, 0)
     event(normed_grad, 1)
@@ -350,7 +351,6 @@
     event(ng_third)
     event(ng_end)
 
-    CH = (zl, zm, zp, z2)
     OWN = {k: (mod(zl + k, 4), mod(z + k, 8) // 4) for k in (4, 3, 2, 1, -1, -2, -3)}
 
     def add3(a, b, c):
@@ -361,8 +361,6 @@
 
     def rs_first(m):
         p = pl.ds(0, HU - NQ[m])
-        for c in range(4):
-            send(("a", m, c), G.at[m, CH[c], diag, p], RY1[m].at[c], "m")
         for c in range(4):
             send(("C", m, c), G.at[m, CH[c], mate, p], RYo[m].at[c], "m")
 

time: 102 us -> 99.2 us (0.973); the launches traced: 100 us -> 99.1 us
  Pallas kernels: 99.7 us -> 98.5 us
    pallas_call x1, Pallas kernels: 97.7 us -> 96.4 us  [per_device(): pl.pallas_call(kernel, out_shape=(sds((64, 2048), bf16), *[sds((2 * HU, 1...]
where the time goes in v4:
time: 99.2 us; the launch traced here: 99.1 us
  Pallas kernels  98.5 us (99%)
    pallas_call x1, Pallas kernels, per_device(): pl.pallas_call(kernel, out_shape=(sds((64, 2048), bf16), *[sds((2 * HU, 1...  96.4 us
    pallas_call x1, Pallas kernels, per_device(): pl.pallas_call(finish, out_shape=(sds((64, 2048), bf16), *[sds((2 * HU, 1...  2.08 us

profile of v4, /device:TPU:6, one launch (start us, length us, event | category | flops | bytes accessed | tf_op | source)
XLA Modules:
  0.0 99.1 jit_solution(3375160489833988181)
XLA Ops:
  0.6 96.4 %ffn_backward.1 = (bf16[64,2048]{1,0:T(8,128)(2,1)}, bf16[704,128]{1,0:T(8,128)(2,1)}, bf16[704,128]{1,0:T(8,128)(2,1)}, bf16[704,128]{1,0:T(8,128)(2,1)}) custom-call(bf16[64,2048]{1,0:T(8,128)(2,1)} %x_hbm.1, f32[1,2048]{1,0:T(1,128)} %bitcast.15, f32[1,2048]{1,0:T(1,128)} %bitcast.16, bf16[704,512]{1,0:T(8,128)(2,1)} %bitcast.10, ...), custom_call_target="tpu_custom_call" | custom-call | tf_op jit(solution)/shard_map/ffn_backward/pallas_call | solution.py:555
  97.0 2.1 %finish.1 = (bf16[64,2048]{1,0:T(8,128)(2,1)}, f32[704,128]{1,0:T(8,128)}, f32[704,128]{1,0:T(8,128)}, f32[704,128]{1,0:T(8,128)}) custom-call(bf16[64,2048]{1,0:T(8,128)(2,1)} %get-tuple-element.12.refs_0_, bf16[704,128]{1,0:T(8,128)(2,1)} %get-tuple-element.13.refs_1_, bf16[704,128]{1,0:T(8,128)(2,1)} %get-tuple-element.14.refs_2_, ...), custom_call_target="tpu_custom_call" | custom-call | tf_op jit(solution)/shard_map/finish/pallas_call | solution.py:566

commit v5 on v4

--- a/solution.py
+++ b/solution.py
@@ -11,16 +11,16 @@
 
 HU = 352
 QU = HU // 2
-NQ = (192, 192, 192)
-N_RECV, N_SEND, N_LOCAL = 108, 48, 20
+NQ = (128, 192, 192)
+N_RECV, N_SEND, N_LOCAL = 108, 64, 20
 ORDER = (
-    2, 3, 21, 0, 38, 47, 12, 1, 30, 4, 5, 22, 23, 25, 16, 40, 8, 6, 39, 24, 9, 14, 32, 26, 46, 27,
-    41, 7, 13, 15, 42, 31, 10, 43, 28, 33, 18, 34, 17, 35, 19, 11, 44, 29, 48, 45, 49, 36, 50, 85,
-    51, 52, 37, 54, 108, 58, 131, 59, 60, 86, 61, 72, 53, 74, 117, 20, 55, 56, 109, 57, 94, 132, 95,
-    76, 71, 118, 120, 87, 122, 62, 64, 110, 124, 78, 119, 133, 123, 67, 125, 63, 88, 101, 97, 99,
-    96, 134, 65, 102, 98, 73, 121, 126, 89, 100, 103, 68, 77, 111, 75, 79, 135, 90, 80, 127, 104,
-    136, 91, 66, 112, 81, 137, 128, 105, 113, 92, 82, 114, 138, 129, 69, 106, 83, 115, 130, 107, 84,
-    70, 139, 116, 93,
+    2, 21, 0, 38, 3, 12, 47, 1, 30, 25, 23, 7, 4, 46, 16, 13, 40, 39, 24, 27, 14, 17, 8, 15, 41, 22,
+    28, 31, 42, 43, 5, 19, 26, 6, 9, 35, 44, 10, 32, 48, 45, 50, 85, 51, 52, 36, 53, 11, 49, 86, 33,
+    72, 62, 18, 37, 71, 74, 34, 58, 131, 59, 54, 108, 55, 87, 56, 57, 73, 94, 60, 76, 61, 132, 20,
+    75, 29, 63, 109, 88, 64, 77, 80, 118, 120, 95, 133, 117, 65, 97, 99, 110, 67, 101, 89, 96, 98,
+    78, 100, 134, 122, 102, 124, 119, 66, 79, 103, 111, 121, 123, 125, 135, 90, 126, 104, 91, 81,
+    136, 112, 68, 127, 105, 137, 113, 92, 82, 128, 106, 114, 83, 138, 69, 129, 107, 115, 84, 130,
+    70, 116, 93, 139,
 )
 
 

time: 99.2 us -> 99.6 us (level)
  no operation moved by 1% of the time
where the time goes in v5:
time: 99.6 us; the launch traced here: 99.5 us
  Pallas kernels  98.9 us (99%)
    pallas_call x1, Pallas kernels, per_device(): pl.pallas_call(kernel, out_shape=(sds((64, 2048), bf16), *[sds((2 * HU, 1...  96.8 us
    pallas_call x1, Pallas kernels, per_device(): pl.pallas_call(finish, out_shape=(sds((64, 2048), bf16), *[sds((2 * HU, 1...  2.08 us

profile of v5, /device:TPU:6, one launch (start us, length us, event | category | flops | bytes accessed | tf_op | source)
XLA Modules:
  0.0 99.5 jit_solution(159948278969829562)
XLA Ops:
  0.6 96.8 %ffn_backward.1 = (bf16[64,2048]{1,0:T(8,128)(2,1)}, bf16[704,128]{1,0:T(8,128)(2,1)}, bf16[704,128]{1,0:T(8,128)(2,1)}, bf16[704,128]{1,0:T(8,128)(2,1)}) custom-call(bf16[64,2048]{1,0:T(8,128)(2,1)} %x_hbm.1, f32[1,2048]{1,0:T(1,128)} %bitcast.15, f32[1,2048]{1,0:T(1,128)} %bitcast.16, bf16[704,512]{1,0:T(8,128)(2,1)} %bitcast.10, ...), custom_call_target="tpu_custom_call" | custom-call | tf_op jit(solution)/shard_map/ffn_backward/pallas_call | solution.py:555
  97.4 2.1 %finish.1 = (bf16[64,2048]{1,0:T(8,128)(2,1)}, f32[704,128]{1,0:T(8,128)}, f32[704,128]{1,0:T(8,128)}, f32[704,128]{1,0:T(8,128)}) custom-call(bf16[64,2048]{1,0:T(8,128)(2,1)} %get-tuple-element.12.refs_0_, bf16[704,128]{1,0:T(8,128)(2,1)} %get-tuple-element.13.refs_1_, bf16[704,128]{1,0:T(8,128)(2,1)} %get-tuple-element.14.refs_2_, ...), custom_call_target="tpu_custom_call" | custom-call | tf_op jit(solution)/shard_map/finish/pallas_call | solution.py:566
